TPU v7x, 32 devices: a whole 2x2x4 slice. The times are simulated.
32 devices in a mesh: ep: 8 (over z, x), tp: 4 (over y, core).
Axes of the slice: x: 2, y: 2, z: 4, core: 2. Of those that a mesh axis runs over, the one named last changes fastest.
Arguments:
- mixer_query: bfloat16 [2048, 2048], P('ep', 'tp'), may hold values from -6 to 6
- mixer_forget: bfloat16 [2048, 2048], P('ep', 'tp'), may hold values from -5.5 to 5.5
- mixer_value: bfloat16 [2048, 2048], P('ep', 'tp'), may hold values from -6 to 6
- mixer_gate: bfloat16 [2048, 2048], P('ep', 'tp'), may hold values from -6 to 6
- forget_floor: float32 [2048], P('tp'), may hold values from 0.88 to 1
- head_gain: float32 [128], replicated, may hold values from 0.1 to 1.9
- mixer_proj: bfloat16 [2048, 2048], P(None, 'tp'), may hold values from -0.125 to 0.125
- expert_tokens: bfloat16 [1024, 2048], P('ep'), may hold values from -6 to 6
- expert_gain: float32 [2048], replicated, may hold values from 0.1 to 1.9
- routes: int32 [1024, 2], P('ep'), may hold values from 0 to 7, as said below
- group_logits: float32 [1024, 4], P('ep'), may hold values from -6 to 6
- choice_logits: float32 [1024, 2], P('ep'), may hold values from -6 to 6
- w_gate: bfloat16 [8, 2048, 2048], P('ep', None, 'tp'), may hold values from -0.125 to 0.125
- w_up: bfloat16 [8, 2048, 2048], P('ep', None, 'tp'), may hold values from -0.125 to 0.125
- w_down: bfloat16 [8, 2048, 2048], P('ep', None, 'tp'), may hold values from -0.125 to 0.125
Outputs:
- mixer_out: bfloat16 [2048, 2048], P('ep', 'tp')
- expert_out: bfloat16 [1024, 2048], P('ep', 'tp')
Inputs may be any that keep to these rules, and one draw needn't show every extreme that they name: `routes`: in each aligned block of 128 rows (the rows of one index of ep) no expert is named by more than 64 rows, and some expert reaches that bound in every block; the 2 experts of a row differ and lie in the same group.
All inputs are finite; a program needn't handle non-finite values.
Results may differ from a plain program's by a relative error of at most 0.01.
Values may be sent and summed in bfloat16 or wider, within the bound.
No kernel may reach another device: no remote copies, remote signals or barrier semaphores. Data moves between devices by JAX's collectives and lax.ppermute only.
A program may use at most 64 MiB of HBM per device.

v0:
```python
import jax
import jax.numpy as jnp
from jax import lax
from jax.sharding import PartitionSpec as P

KEYDIM = 128
VDIM = 128
GROUPS = 4
TOPK = 2
BLOCK = 64


norm_eps = 1e-06
highest_precision = lax.Precision.HIGHEST


def entering(shard, axis, join, neutral):
    place = lax.axis_index(axis)
    gathered = jax.tree.map(
        lambda a, kind: lax.all_gather(a.astype(kind), axis), shard, (jnp.bfloat16, jnp.bfloat16)
    )
    state = jax.tree.map(lambda a, e: jnp.zeros_like(a) + jnp.asarray(e, a.dtype), shard, neutral)

    def one(lap, state):
        return join(
            state,
            jax.tree.map(
                lambda a, own: lax.dynamic_index_in_dim(a, lap, 0, False).astype(own.dtype),
                gathered,
                shard,
            ),
        )

    return lax.fori_loop(0, place, one, state)


def rms_scale(features, gain_vec):
    return (
        features
        * lax.rsqrt(jnp.mean(features * features, axis=-1, keepdims=True) + norm_eps)
        * gain_vec
    )


def block_terms(query_block, input_block, log_blk, value_block, carried_state):
    cumulative_log = jnp.cumsum(log_blk, axis=0)
    between_block_term = jnp.einsum(
        "zug,ugr->zur",
        query_block * jnp.exp(cumulative_log),
        carried_state,
        precision=highest_precision,
    )
    causal = jnp.tril(jnp.ones((query_block.shape[0], query_block.shape[0]), dtype=bool))[
        :, :, None, None
    ]
    differ = cumulative_log[:, None] - cumulative_log[None, :]
    decays = jnp.exp(jnp.where(causal, differ, -jnp.inf))
    scores = jnp.sum(query_block[:, None] * input_block[None, :] * decays, axis=-1)
    result = between_block_term + jnp.einsum(
        "tsh,shv->thv", scores, value_block, precision=highest_precision
    )
    ending_log_decay = cumulative_log[-1]
    updated_state = jnp.exp(ending_log_decay)[..., None] * carried_state + jnp.einsum(
        "twa,twr->war",
        input_block * jnp.exp(ending_log_decay[None] - cumulative_log),
        value_block,
        precision=highest_precision,
    )
    return (updated_state, result, cumulative_log)


def mixer_local(
    mixer_query, mixer_forget, mixer_value, mixer_gate, forget_floor, head_gain, mixer_proj
):
    length = mixer_query.shape[0]
    heads_local = mixer_query.shape[1] // KEYDIM
    blocks = length // BLOCK

    def split_blocks(source_array, last_width):
        return source_array.reshape(blocks, BLOCK, heads_local, last_width)

    queries = jax.nn.silu(mixer_query.astype(jnp.float32))
    input_rates = (1.0 - forget_floor) * jax.nn.sigmoid(-mixer_forget.astype(jnp.float32))
    log_forget = jnp.log1p(-input_rates)
    value_rows = mixer_value.astype(jnp.float32)

    def advance(carry_pair, block_inputs):
        carried_state, offset_log = carry_pair
        query_block, input_block, value_block, log_blk = block_inputs
        updated_state, result, cumulative_log = block_terms(
            query_block, input_block, log_blk, value_block, carried_state
        )
        scaled_values = query_block * jnp.exp(cumulative_log + offset_log[None])
        return ((updated_state, offset_log + cumulative_log[-1]), (result, scaled_values))

    initial = (
        jnp.zeros((heads_local, KEYDIM, VDIM), jnp.float32),
        jnp.zeros((heads_local, KEYDIM), jnp.float32),
    )
    (local_state, total_log), (output_rows, scaled_values) = lax.scan(
        advance,
        initial,
        (
            split_blocks(queries, KEYDIM),
            split_blocks(input_rates, KEYDIM),
            split_blocks(value_rows, VDIM),
            split_blocks(log_forget, KEYDIM),
        ),
    )

    def combine(earlier, later):
        return (earlier[0] * later[0], later[0][..., None] * earlier[1] + later[1])

    identity = (jnp.ones_like(total_log), jnp.zeros_like(local_state))
    incoming_state = entering((jnp.exp(total_log), local_state), "ep", combine, identity)
    output_rows = output_rows + jnp.einsum(
        "qsfa,fap->qsfp", scaled_values, incoming_state[1], precision=highest_precision
    )
    output_rows = output_rows.reshape(length, heads_local, VDIM)
    gate_act = jax.nn.silu(mixer_gate.astype(jnp.float32)).reshape(length, heads_local, VDIM)
    gated_out = rms_scale(output_rows, head_gain) * gate_act
    mixed_heads = gated_out.reshape(length, heads_local * VDIM).astype(jnp.bfloat16)
    summed = jnp.dot(
        lax.all_gather(mixed_heads, "tp", axis=1, tiled=True),
        mixer_proj,
        preferred_element_type=jnp.float32,
    )
    return summed.astype(jnp.bfloat16)


def gate_weights(routes, group_logits, choice_logits, group_size):
    group_exp = jnp.exp(group_logits)
    group_prob = group_exp / jnp.sum(group_exp, axis=-1, keepdims=True)
    groups_of = routes // group_size
    member = (groups_of[..., None] == jnp.arange(GROUPS, dtype=jnp.int32)).astype(jnp.float32)
    picked_prob = jnp.sum(member * group_prob[:, None, :], axis=-1)
    choice_exp = jnp.exp(choice_logits)
    together = (groups_of[:, :, None] == groups_of[:, None, :]).astype(jnp.float32)
    within = jnp.sum(together * choice_exp[:, None, :], axis=-1)
    return picked_prob * choice_exp / within


def finish(gate_pre, up_pre, down_local, sources, slot_count):
    hidden = (jax.nn.silu(gate_pre) * up_pre).astype(jnp.bfloat16)
    summed = jnp.dot(
        lax.all_gather(hidden, "tp", axis=1, tiled=True),
        down_local,
        preferred_element_type=jnp.float32,
    )
    shaped = summed.astype(jnp.bfloat16).reshape(sources, slot_count, down_local.shape[1])
    return lax.all_to_all(shaped, "ep", split_axis=0, concat_axis=0, tiled=True)


def expert_local(
    expert_tokens, expert_gain, routes, group_logits, choice_logits, w_gate, w_up, w_down
):
    count_rows, model_width = expert_tokens.shape
    experts_all = lax.axis_size("ep")
    capacity = 2 * TOPK * count_rows // experts_all
    normed = rms_scale(expert_tokens.astype(jnp.float32), expert_gain).astype(jnp.bfloat16)
    weights = gate_weights(routes, group_logits, choice_logits, experts_all // GROUPS)
    flat_routes = routes.reshape(-1)
    onehot = (flat_routes[:, None] == jnp.arange(experts_all, dtype=jnp.int32)).astype(jnp.int32)
    earlier = jnp.cumsum(onehot, axis=0) - onehot
    ranks = jnp.sum(earlier * onehot, axis=-1)
    slot_of = flat_routes * capacity + ranks
    token_ids = jnp.arange(flat_routes.shape[0], dtype=jnp.int32) // TOPK
    token_of = jnp.full((experts_all * capacity,), count_rows, jnp.int32).at[slot_of].set(token_ids)
    padded = jnp.concatenate([normed, jnp.zeros((1, model_width), jnp.bfloat16)], axis=0)
    outgoing = padded[token_of].reshape(experts_all, capacity, model_width)
    gate_local = w_gate[0]
    up_local = w_up[0]
    down_local = w_down[0]
    arrived = lax.all_to_all(outgoing, "ep", split_axis=0, concat_axis=0, tiled=True)
    sources, slot_count, _ = arrived.shape
    flat_in = arrived.reshape(sources * slot_count, model_width)
    gate_pre = jnp.dot(flat_in, gate_local, preferred_element_type=jnp.float32)
    up_pre = jnp.dot(flat_in, up_local, preferred_element_type=jnp.float32)
    came_back = finish(gate_pre, up_pre, down_local, sources, slot_count)
    picked = (
        came_back.reshape(-1, came_back.shape[-1])[slot_of].astype(jnp.float32)
        * weights.reshape(-1)[:, None]
    )
    return jnp.sum(picked.reshape(count_rows, TOPK, -1), axis=1).astype(jnp.bfloat16)


def per_device(
    mixer_query,
    mixer_forget,
    mixer_value,
    mixer_gate,
    forget_floor,
    head_gain,
    mixer_proj,
    expert_tokens,
    expert_gain,
    routes,
    group_logits,
    choice_logits,
    w_gate,
    w_up,
    w_down,
):
    mixer_out = mixer_local(
        mixer_query, mixer_forget, mixer_value, mixer_gate, forget_floor, head_gain, mixer_proj
    )
    expert_out = expert_local(
        expert_tokens, expert_gain, routes, group_logits, choice_logits, w_gate, w_up, w_down
    )
    return (mixer_out, expert_out)


def solution(mesh):
    return jax.shard_map(
        per_device,
        mesh=mesh,
        in_specs=(
            P("ep", "tp"),
            P("ep", "tp"),
            P("ep", "tp"),
            P("ep", "tp"),
            P("tp"),
            P(),
            P(None, "tp"),
            P("ep", None),
            P(),
            P("ep", None),
            P("ep", None),
            P("ep", None),
            P("ep", None, "tp"),
            P("ep", None, "tp"),
            P("ep", None, "tp"),
        ),
        out_specs=(P("ep", "tp"), P("ep", "tp")),
        check_vma=False,
    )
```

profile of v0, /device:TPU:0, one launch (start us, length us, event | category | flops | bytes accessed | tf_op | source)
XLA Modules:
  0.0 168.5 jit_solution(13482604115918556136)
XLA Ops:
  10.3 1.4 scatter_custom_fusion
  13.0 1.2 fusion.35
  14.3 3.3 %gather_fusion = bf16[512,2048]{1,0:T(8,128)(2,1)} fusion(bf16[129,2048]{1,0:T(8,128)(2,1)S(1)} %concatenate.3, s32[1024]{0:T(1024)S(1)} %pad_clamp_fusion.1), kind=kCustom, calls=%fused_computation | custom fusion | bytes 4196352 | tf_op jit(solution)/shard_map/gather | solution.py:170
  17.6 7.4 %all-to-all-start = ((bf16[8,64,2048]{2,1,0:T(8,128)(2,1)}), bf16[8,64,2048]{2,1,0:T(8,128)(2,1)}, u32[]{:S(2)}, u32[]{:S(2)}) async-start(bf16[8,64,2048]{2,1,0:T(8,128)(2,1)} %bitcast.133), calls=%async_computation | async-start | bytes 4194304 | tf_op jit(solution)/shard_map/all_to_all | solution.py:174
  25.1 1.2 divide_multiply_fusion
  29.6 1.9 %reshape.178 = f32[4,64,4,128]{3,2,1,0:T(4,128)} reshape(bf16[256,512]{1,0:T(8,128)(2,1)} %param.21) | data formatting | bytes 786432 | tf_op jit(solution)/shard_map/reshape | solution.py:80
  31.5 37.6 %while.30 = (s32[]{:T(128)}, f32[4,128,128]{2,1,0:T(8,128)S(1)}, f32[4,128]{1,0:T(4,128)S(1)}, f32[4,64,4,128]{3,1,0,2:T(8,128)}, f32[4,64,4,128]{3,1,0,2:T(8,12...) while((s32[]{:T(128)}, f32[4,128,128]{2,1,0:T(8,128)S(1)}, ...), condition=%wide.region_3.4_spmd.clone, body=%wide.region_0.3_spmd.clone.sunk | while | flops 138826752 | bytes 5011073 | solution.py:100
  33.5 3.7 %multiply_reduce_fusion.4 = f32[64,64,4]{1,2,0:T(4,128)S(1)} fusion(f32[64,4,128]{2,0,1:T(8,128)S(1)} %copy.120, f32[64,4,128]{2,1,0:T(4,128)S(1)} %fusion.74, f32[64,4,128]{2,0,1:T(8,128)S(1)} %copy.121, f32[64,4,128]{2,1,0:T(4,128)S(1)} %get-tuple-element.314, pred[64,64]{1,0:T(8,128)(4,1)S(1)} %iota_compare_fusion.5), kind=kLoop, calls=%fused_computation.5.clone.1 | loop fusion | flops 10469376 | bytes 593920 | tf_op jit(solution)/shard_map/while/body/eval_jaxpr/reduce_sum | solution.py:58
  42.9 3.7 %multiply_reduce_fusion.4 = f32[64,64,4]{1,2,0:T(4,128)S(1)} fusion(f32[64,4,128]{2,0,1:T(8,128)S(1)} %copy.120, f32[64,4,128]{2,1,0:T(4,128)S(1)} %fusion.74, f32[64,4,128]{2,0,1:T(8,128)S(1)} %copy.121, f32[64,4,128]{2,1,0:T(4,128)S(1)} %get-tuple-element.314, pred[64,64]{1,0:T(8,128)(4,1)S(1)} %iota_compare_fusion.5), kind=kLoop, calls=%fused_computation.5.clone.1 | loop fusion | flops 10469376 | bytes 593920 | tf_op jit(solution)/shard_map/while/body/eval_jaxpr/reduce_sum | solution.py:58
  52.3 3.7 %multiply_reduce_fusion.4 = f32[64,64,4]{1,2,0:T(4,128)S(1)} fusion(f32[64,4,128]{2,0,1:T(8,128)S(1)} %copy.120, f32[64,4,128]{2,1,0:T(4,128)S(1)} %fusion.74, f32[64,4,128]{2,0,1:T(8,128)S(1)} %copy.121, f32[64,4,128]{2,1,0:T(4,128)S(1)} %get-tuple-element.314, pred[64,64]{1,0:T(8,128)(4,1)S(1)} %iota_compare_fusion.5), kind=kLoop, calls=%fused_computation.5.clone.1 | loop fusion | flops 10469376 | bytes 593920 | tf_op jit(solution)/shard_map/while/body/eval_jaxpr/reduce_sum | solution.py:58
  61.7 3.7 %multiply_reduce_fusion.4 = f32[64,64,4]{1,2,0:T(4,128)S(1)} fusion(f32[64,4,128]{2,0,1:T(8,128)S(1)} %copy.120, f32[64,4,128]{2,1,0:T(4,128)S(1)} %fusion.74, f32[64,4,128]{2,0,1:T(8,128)S(1)} %copy.121, f32[64,4,128]{2,1,0:T(4,128)S(1)} %get-tuple-element.314, pred[64,64]{1,0:T(8,128)(4,1)S(1)} %iota_compare_fusion.5), kind=kLoop, calls=%fused_computation.5.clone.1 | loop fusion | flops 10469376 | bytes 593920 | tf_op jit(solution)/shard_map/while/body/eval_jaxpr/reduce_sum | solution.py:58
  69.8 3.5 %all-to-all-done = bf16[8,64,2048]{2,1,0:T(8,128)(2,1)} async-done(((bf16[8,64,2048]{2,1,0:T(8,128)(2,1)}), bf16[8,64,2048]{2,1,0:T(8,128)(2,1)}, u32[]{:S(2)}, u32[]{:S(2)}) %all-to-all-start) | async-done | bytes 2097184 | tf_op jit(solution)/shard_map/all_to_all | solution.py:174
  73.3 3.0 %fusion.22 = f32[512,512]{1,0:T(8,128)S(1)} fusion(bf16[512,2048]{1,0:T(8,128)(2,1)} %bitcast.15, bf16[1,2048,512]{2,1,0:T(8,128)(2,1)S(1)} %copy-done), kind=kOutput, calls=%fused_computation.42 | convolution fusion | flops 1073741824 | bytes 5242880 | tf_op jit(solution)/shard_map/dot_general | solution.py:177
  76.3 3.7 %fusion.30 = bf16[512,512]{1,0:T(8,128)(2,1)} fusion(bf16[512,2048]{1,0:T(8,128)(2,1)} %bitcast.15, bf16[1,2048,512]{2,1,0:T(8,128)(2,1)S(1)} %copy-done.7, f32[512,512]{1,0:T(8,128)S(1)} %fusion.22), kind=kOutput, calls=%fused_computation.48 | convolution fusion | flops 1075314688 | bytes 5767168 | tf_op jit(solution)/shard_map/dot_general | solution.py:178
  80.2 18.7 %all-gather.2 = bf16[8,4,128]{2,1,0:T(4,128)(2,1)S(1)} all-gather(bf16[1,4,128]{2,1,0:T(4,128)(2,1)S(1)} %fusion.49), channel_id=2, replica_groups=mesh['ep'=8,'tp'=4] {'ep'}, dimensions={0}, use_global_device_ids=true | all-gather | bytes 9216 | tf_op jit(solution)/shard_map/all_gather | solution.py:20
  98.8 12.7 %all-gather.11.cloned.1.call-done = bf16[32,128,128]{2,1,0:T(8,128)(2,1)} async-done(((bf16[4,128,128]{2,1,0:T(8,128)(2,1)}), bf16[32,128,128]{2,1,0:T(8,128)(2,1)}) %all-gather.11.cloned.1.call-update) | async-done | bytes 1048592 | tf_op jit(solution)/shard_map/all_gather | solution.py:20
  111.6 1.7 %fusion.52 = f32[4,128,256]{1,2,0:S(1)} fusion(f32[4,128,128]{2,1,0:T(8,128)S(1)} %get-tuple-element.99, f32[4,128,256]{1,2,0:T(8,128)} %bitcast.138), kind=kOutput, calls=%fused_computation.106 | convolution fusion | flops 201326592 | bytes 1310720
  115.3 19.1 %all-gather.9.cloned.1.call-done = bf16[512,2048]{1,0:T(8,128)(2,1)} async-done(((bf16[512,512]{1,0:T(8,128)(2,1)}), bf16[512,2048]{1,0:T(8,128)(2,1)}) %all-gather.9.cloned.1.call-update) | async-done | bytes 2097168 | tf_op jit(solution)/shard_map/all_gather | solution.py:146
  134.4 4.3 %fusion.27 = bf16[512,512]{1,0:T(8,128)(2,1)} fusion(bf16[512,2048]{1,0:T(8,128)(2,1)} %all-gather.9.cloned.1.call-done, bf16[1,2048,512]{2,1,0:T(8,128)(2,1)} %param.33), kind=kOutput, calls=%fused_computation.47 | convolution fusion | flops 1074003968 | bytes 4718592 | tf_op jit(solution)/shard_map/dot_general | solution.py:145
  138.7 5.5 %all-to-all-start.1 = ((bf16[8,64,512]{2,1,0:T(8,128)(2,1)}), bf16[8,64,512]{2,1,0:T(8,128)(2,1)S(1)}, u32[]{:S(2)}, u32[]{:S(2)}) async-start(bf16[8,64,512]{2,1,0:T(8,128)(2,1)} %bitcast.19), calls=%async_computation.1 | async-start | bytes 1048576 | tf_op jit(solution)/shard_map/all_to_all | solution.py:151
  144.4 8.9 %all-gather.7.cloned.1.call-done = bf16[256,2048]{1,0:T(8,128)(2,1)} async-done(((bf16[256,512]{1,0:T(8,128)(2,1)}), bf16[256,2048]{1,0:T(8,128)(2,1)}) %all-gather.7.cloned.1.call-update) | async-done | bytes 1048592 | tf_op jit(solution)/shard_map/all_gather | solution.py:124
  153.3 3.3 %convolution_convert_fusion = bf16[256,512]{1,0:T(8,128)(2,1)} fusion(bf16[256,2048]{1,0:T(8,128)(2,1)} %all-gather.7.cloned.1.call-done, bf16[2048,512]{1,0:T(8,128)(2,1)} %param.25), kind=kOutput, calls=%fused_computation.49 | convolution fusion | flops 537001984 | bytes 3407872 | tf_op jit(solution)/shard_map/dot_general | solution.py:123
  156.7 2.4 %all-to-all-done.1 = bf16[8,64,512]{2,1,0:T(8,128)(2,1)S(1)} async-done(((bf16[8,64,512]{2,1,0:T(8,128)(2,1)}), bf16[8,64,512]{2,1,0:T(8,128)(2,1)S(1)}, u32[]{:S(2)}, u32[]{:S(2)}) %all-to-all-start.1) | async-done | bytes 524320 | tf_op jit(solution)/shard_map/all_to_all | solution.py:151
  160.6 1.4 multiply_reduce_fusion.1
  (119 shorter events, 34.6 us)
Async XLA Ops:
  7.2 66.2 %copy-start = (bf16[1,2048,512]{2,1,0:T(8,128)(2,1)S(1)}, bf16[1,2048,512]{2,1,0:T(8,128)(2,1)}, u32[]{:S(2)}) copy-start(bf16[1,2048,512]{2,1,0:T(8,128)(2,1)} %param.31) | copy-start | bytes 6291460
  17.6 7.5 %copy-start.5 = (f32[512]{0:T(512)S(1)}, f32[512]{0:T(512)}, u32[]{:S(2)}) copy-start(f32[512]{0:T(512)} %param.23) | copy-start | bytes 6148
  17.6 55.8 %all-to-all-start = ((bf16[8,64,2048]{2,1,0:T(8,128)(2,1)}), bf16[8,64,2048]{2,1,0:T(8,128)(2,1)}, u32[]{:S(2)}, u32[]{:S(2)}) async-start(bf16[8,64,2048]{2,1,0:T(8,128)(2,1)} %bitcast.133), calls=%async_computation | async-start | bytes 4194304 | tf_op jit(solution)/shard_map/all_to_all | solution.py:174
  25.0 86.6 %all-gather.11.cloned.1.call-start = ((), (), s32[]{:S(2)}) async-start(), calls=%async_computation.4 | async-start | bytes 1179648 | tf_op jit(solution)/shard_map/all_gather | solution.py:20
  69.8 64.7 %all-gather.9.cloned.1.call-start = ((), (), s32[]{:S(2)}) async-start(), calls=%async_computation.3 | async-start | bytes 2621440 | tf_op jit(solution)/shard_map/all_gather | solution.py:146
  73.3 3.0 %copy-start.7 = (bf16[1,2048,512]{2,1,0:T(8,128)(2,1)S(1)}, bf16[1,2048,512]{2,1,0:T(8,128)(2,1)}, u32[]{:S(2)}) copy-start(bf16[1,2048,512]{2,1,0:T(8,128)(2,1)} %param.32) | copy-start | bytes 6291460
  76.3 22.5 %copy-start.6 = (f32[128]{0:T(128)S(1)}, f32[128]{0:T(128)}, u32[]{:S(2)}) copy-start(f32[128]{0:T(128)} %param.24) | copy-start | bytes 1540
  80.1 73.2 %all-gather.7.cloned.1.call-start = ((), (), s32[]{:S(2)}) async-start(), calls=%async_computation.2 | async-start | bytes 1310720 | tf_op jit(solution)/shard_map/all_gather | solution.py:124
  111.6 1.7 %copy-start.1 = (f32[4,64,4,128]{3,1,0,2:T(8,128)S(1)}, f32[4,64,4,128]{3,1,0,2:T(8,128)}, u32[]{:S(2)}) copy-start(f32[4,64,4,128]{3,1,0,2:T(8,128)} %get-tuple-element.96) | copy-start | bytes 1572868
  111.6 2.8 %copy-start.2 = (bf16[256,512]{1,0:T(8,128)(2,1)S(1)}, bf16[256,512]{1,0:T(8,128)(2,1)}, u32[]{:S(2)}) copy-start(bf16[256,512]{1,0:T(8,128)(2,1)} %param.22) | copy-start | bytes 786436
  113.5 1.8 %copy-start.3 = (f32[128,4]{0,1:T(4,128)S(1)}, f32[128,4]{0,1:T(4,128)}, u32[]{:S(2)}) copy-start(f32[128,4]{0,1:T(4,128)} %param.29) | copy-start | bytes 6148
  115.3 28.9 %copy-start.4 = (f32[128,2]{0,1:T(2,128)S(1)}, f32[128,2]{0,1:T(2,128)}, u32[]{:S(2)}) copy-start(f32[128,2]{0,1:T(2,128)} %param.30) | copy-start | bytes 3076
  138.7 20.4 %all-to-all-start.1 = ((bf16[8,64,512]{2,1,0:T(8,128)(2,1)}), bf16[8,64,512]{2,1,0:T(8,128)(2,1)S(1)}, u32[]{:S(2)}, u32[]{:S(2)}) async-start(bf16[8,64,512]{2,1,0:T(8,128)(2,1)} %bitcast.19), calls=%async_computation.1 | async-start | bytes 1048576 | tf_op jit(solution)/shard_map/all_to_all | solution.py:151
Sparse Core Ops, SparseCore 0:
  69.9 41.6 all-gather.10
  113.1 21.2 all-gather.8
  136.6 16.7 all-gather.6
where the time goes:
time: 169 us; the launch traced here: 168 us
  waiting for transfers between devices  46.7 us (28%)
  other arithmetic  36.4 us (22%)
  matrix products  23.7 us (14%)
  blocking collectives  18.7 us (11%)
  local copies, waits for them, and re-layouts  15.7 us (9%)
  between operations  14 us (8%)
  starting transfers between devices  13 us (8%)
    all_gather x1, waiting for transfers between devices, finish(): lax.all_gather(hidden, 'tp', axis=1, tiled=True)  19.1 us
    all_gather x1, blocking collectives, entering(): lax.all_gather(a.astype(kind), axis)  18.7 us
    reduce_sum x4, other arithmetic, block_terms(): jnp.sum(query_block[:, None] * input_block[None, :] * decays, axis=-1)  14.9 us
    all_gather x1, waiting for transfers between devices, entering(): lax.all_gather(a.astype(kind), axis)  12.7 us
    all_gather x1, waiting for transfers between devices, mixer_local(): lax.all_gather(mixed_heads, 'tp', axis=1, tiled=True)  8.91 us
    all_to_all x1, starting transfers between devices, expert_local(): lax.all_to_all(outgoing, 'ep', split_axis=0, concat_axis=0, tiled=True)  7.41 us
    all_to_all x1, starting transfers between devices, finish(): return lax.all_to_all(shaped, 'ep', split_axis=0, concat_axis=0, tiled=True)  5.51 us
    dot_general x1, matrix products, finish(): jnp.dot(lax.all_gather(hidden, 'tp', axis=1, tiled=True), down_local, pre...  4.26 us
  transfers between devices with their start and end apart: 5, of which 5 were waited for; matrix products, arithmetic and copies ran while one was open for 37% of the time, Pallas kernels for 0%

commit v1 on v0

v1 whole, which is shorter than its diff:
```python
import functools

import jax
import jax.numpy as jnp
from jax import lax
from jax.experimental import pallas as pl
from jax.experimental.pallas import tpu as pltpu
from jax.sharding import PartitionSpec as P

KEYDIM = 128
VDIM = 128
GROUPS = 4
TOPK = 2

norm_eps = 1e-06
f32 = jnp.float32
bf16 = jnp.bfloat16


def dot(a, b, ca, cb):
    return lax.dot_general(a, b, (((ca,), (cb,)), ((), ())), preferred_element_type=f32)


def silu(v):
    return v / (1.0 + jnp.exp(-v))


def mixer_scan_kernel(query, forget, value, floor, out, entry_query, state, decay):
    length = query.shape[0]
    queries = silu(query[...].astype(f32))
    rates = (1.0 - floor[...]) / (1.0 + jnp.exp(forget[...].astype(f32)))
    logs = jnp.log(1.0 - rates)
    high = logs.astype(bf16)
    low = (logs - high.astype(f32)).astype(bf16)
    rows = lax.broadcasted_iota(jnp.int32, (length, length), 0)
    cols = lax.broadcasted_iota(jnp.int32, (length, length), 1)
    causal = rows >= cols
    ones = jnp.where(causal, 1.0, 0.0).astype(bf16)
    cumulative = dot(ones, high, 1, 0) + dot(ones, low, 1, 0)
    total = cumulative[length - 1 :, :]
    centred = cumulative - 0.5 * total
    grown = jnp.exp(centred)
    values = value[...]
    left = (queries * grown).astype(bf16)
    right = (rates * jnp.exp(-centred)).astype(bf16)
    scores = jnp.where(causal, dot(left, right, 1, 1), 0.0).astype(bf16)
    out[...] = dot(scores, values, 1, 0)
    entry_query[...] = (queries * jnp.exp(cumulative)).astype(bf16)
    kept = (rates * jnp.exp(total - cumulative)).astype(bf16)
    state[0] = dot(values, kept, 0, 0).astype(bf16)
    decay[0] = jnp.exp(total).astype(bf16)


def mixer_scan(query, forget, value, floor):
    length, width = query.shape
    heads = width // KEYDIM
    block = pl.BlockSpec((length, KEYDIM), lambda h: (0, h))
    return pl.pallas_call(
        mixer_scan_kernel,
        grid=(heads,),
        in_specs=[block, block, block, pl.BlockSpec((1, KEYDIM), lambda h: (0, h))],
        out_specs=[
            block,
            block,
            pl.BlockSpec((1, VDIM, KEYDIM), lambda h: (h, 0, 0)),
            pl.BlockSpec((1, 1, KEYDIM), lambda h: (h, 0, 0)),
        ],
        out_shape=[
            jax.ShapeDtypeStruct((length, width), f32),
            jax.ShapeDtypeStruct((length, width), bf16),
            jax.ShapeDtypeStruct((heads, VDIM, KEYDIM), bf16),
            jax.ShapeDtypeStruct((heads, 1, KEYDIM), bf16),
        ],
        name="mixer_scan",
    )(query, forget, value, floor.reshape(1, width))


def prefix_kernel(states, decays, out):
    parts, rows, _ = states.shape
    heads = decays.shape[1]
    per_head = rows // heads
    head_of = lax.broadcasted_iota(jnp.int32, (rows, KEYDIM), 0)
    acc = jnp.zeros((rows, KEYDIM), f32)
    for part in range(parts):
        out[part] = acc.astype(bf16)
        if part + 1 < parts:
            shrink = decays[part].astype(f32)
            spread = jnp.broadcast_to(shrink[0:1], (rows, KEYDIM))
            for head in range(1, heads):
                spread = jnp.where(head_of >= head * per_head, shrink[head : head + 1], spread)
            acc = spread * acc + states[part].astype(f32)


def entering_states(state, decay):
    parts = lax.axis_size("ep")
    heads = state.shape[0]
    rows = VDIM // parts
    sliced = state.reshape(heads, parts, rows, KEYDIM).transpose(1, 0, 2, 3)
    sliced = sliced.reshape(parts, heads * rows, KEYDIM)
    tail = jnp.broadcast_to(decay.reshape(1, heads, KEYDIM), (parts, heads, KEYDIM))
    packed = jnp.concatenate([sliced, tail], axis=1)
    packed = lax.all_to_all(packed, "ep", split_axis=0, concat_axis=0, tiled=True)
    prefixes = pl.pallas_call(
        prefix_kernel,
        out_shape=jax.ShapeDtypeStruct((parts, heads * rows, KEYDIM), bf16),
        name="state_prefix",
    )(packed[:, : heads * rows], packed[:, heads * rows :])
    back = lax.all_to_all(prefixes, "ep", split_axis=0, concat_axis=0, tiled=True)
    back = back.reshape(parts, heads, rows, KEYDIM).transpose(1, 0, 2, 3)
    return back.reshape(heads, VDIM, KEYDIM)


def mixer_gate_kernel(local, entry_query, entering, gate, gain, out):
    recurrent = local[...] + dot(entry_query[...], entering[0], 1, 1)
    mean = jnp.mean(recurrent * recurrent, axis=-1, keepdims=True)
    scaled = recurrent * lax.rsqrt(mean + norm_eps) * gain[...]
    out[...] = (scaled * silu(gate[...].astype(f32))).astype(bf16)


def mixer_gated(local, entry_query, entering, gate, gain):
    length, width = local.shape
    block = pl.BlockSpec((length, VDIM), lambda h: (0, h))
    return pl.pallas_call(
        mixer_gate_kernel,
        grid=(width // VDIM,),
        in_specs=[
            block,
            block,
            pl.BlockSpec((1, VDIM, KEYDIM), lambda h: (h, 0, 0)),
            block,
            pl.BlockSpec((1, VDIM), lambda h: (0, 0)),
        ],
        out_specs=block,
        out_shape=jax.ShapeDtypeStruct((length, width), bf16),
        name="mixer_gated",
    )(local, entry_query, entering, gate, gain.reshape(1, VDIM))


def four_parts_kernel(place, own, beside, across, w0, w1, w2, w3, out):
    width = own.shape[1]
    acc = dot(own[...], w0[...], 1, 0)
    acc += dot(beside[...], w1[...], 1, 0)
    acc += dot(across[:, :width], w2[...], 1, 0)
    acc += dot(across[:, width:], w3[...], 1, 0)
    out[...] = acc.astype(bf16)


def spread_dot(part, weight):
    size = lax.axis_size("tp")
    if size != 4:
        full = lax.all_gather(part, "tp", axis=1, tiled=True)
        return jnp.dot(full, weight, preferred_element_type=f32).astype(bf16)
    count, width = part.shape
    columns = weight.shape[1]
    beside = lax.ppermute(part, "tp", [(i, i ^ 2) for i in range(size)])
    pair = jnp.concatenate([part, beside], axis=1)
    across = lax.ppermute(pair, "tp", [(i, i ^ 1) for i in range(size)])
    place = lax.axis_index("tp").astype(jnp.int32).reshape(1)
    whole = lambda cols: pl.BlockSpec((count, cols), lambda i, p: (0, 0))
    rows = lambda flip: pl.BlockSpec((width, columns), lambda i, p: (p[0] ^ flip, 0))
    return pl.pallas_call(
        four_parts_kernel,
        grid_spec=pltpu.PrefetchScalarGridSpec(
            num_scalar_prefetch=1,
            grid=(1,),
            in_specs=[whole(width), whole(width), whole(2 * width)]
            + [rows(flip) for flip in (0, 2, 1, 3)],
            out_specs=pl.BlockSpec((count, columns), lambda i, p: (0, 0)),
        ),
        out_shape=jax.ShapeDtypeStruct((count, columns), bf16),
        name="spread_dot",
    )(place, part, beside, across, weight, weight, weight, weight)


def slot_ranks(routes, experts):
    tokens = routes.shape[1]
    expert = lax.broadcasted_iota(jnp.int32, (experts, tokens), 0)
    named = [routes[j : j + 1, :] == expert for j in range(TOPK)]
    member = functools.reduce(jnp.logical_or, named)
    before = lax.broadcasted_iota(jnp.int32, (tokens, tokens), 0)
    token = lax.broadcasted_iota(jnp.int32, (tokens, tokens), 1)
    earlier = jnp.where(before < token, 1.0, 0.0).astype(bf16)
    counts = dot(jnp.where(member, 1.0, 0.0).astype(bf16), earlier, 1, 0)
    return named, jnp.where(member, counts.astype(jnp.int32), -1)


def dispatch_kernel(place, tokens, gain, routes, out, *, capacity):
    features = tokens[...].astype(f32)
    scale = lax.rsqrt(jnp.mean(features * features, axis=-1, keepdims=True) + norm_eps)
    normed = (features * scale * gain[...]).astype(bf16)
    half = out.shape[1]
    mine = jnp.where(place[0] == 0, normed[:, :half], normed[:, half:])
    experts = out.shape[0] // capacity
    _, ranks = slot_ranks(routes[...], experts)
    slot = lax.broadcasted_iota(jnp.int32, (capacity, tokens.shape[0]), 0)
    for e in range(experts):
        pick = jnp.where(ranks[e : e + 1, :] == slot, 1.0, 0.0).astype(bf16)
        out[e * capacity : (e + 1) * capacity, :] = dot(pick, mine, 1, 0).astype(bf16)


def combine_kernel(routes, group_logits, choice_logits, values, out, *, capacity):
    experts = values.shape[0] // capacity
    tokens = routes.shape[1]
    chosen = routes[...]
    named, ranks = slot_ranks(chosen, experts)
    group_exp = jnp.exp(group_logits[...])
    group_prob = group_exp / jnp.sum(group_exp, axis=0, keepdims=True)
    choice_exp = jnp.exp(choice_logits[...])
    size = experts // GROUPS
    groups_of = [lax.div(chosen[j : j + 1, :], jnp.int32(size)) for j in range(TOPK)]
    spread = jnp.zeros((experts, tokens), f32)
    for j in range(TOPK):
        prob = jnp.zeros((1, tokens), f32)
        for g in range(GROUPS):
            prob = jnp.where(groups_of[j] == g, group_prob[g : g + 1, :], prob)
        within = jnp.zeros((1, tokens), f32)
        for i in range(TOPK):
            within += jnp.where(groups_of[i] == groups_of[j], choice_exp[i : i + 1, :], 0.0)
        weight = prob * choice_exp[j : j + 1, :] / within
        spread = jnp.where(named[j], weight, spread)
    slot = lax.broadcasted_iota(jnp.int32, (capacity, tokens), 0)
    mix = jnp.concatenate(
        [
            jnp.where(ranks[e : e + 1, :] == slot, spread[e : e + 1, :], 0.0)
            for e in range(experts)
        ],
        axis=0,
    )
    high = mix.astype(bf16)
    low = (mix - high.astype(f32)).astype(bf16)
    out[...] = (dot(high, values[...], 0, 0) + dot(low, values[...], 0, 0)).astype(bf16)


def expert_dispatch(expert_tokens, expert_gain, routes):
    count, width = expert_tokens.shape
    experts = lax.axis_size("ep")
    capacity = 2 * TOPK * count // experts
    half = width // 2
    core = (lax.axis_index("tp") % 2).astype(jnp.int32).reshape(1)
    vmem = pl.BlockSpec(memory_space=pltpu.VMEM)
    outgoing = pl.pallas_call(
        functools.partial(dispatch_kernel, capacity=capacity),
        in_specs=[pl.BlockSpec(memory_space=pltpu.SMEM), vmem, vmem, vmem],
        out_specs=vmem,
        out_shape=jax.ShapeDtypeStruct((experts * capacity, half), bf16),
        name="expert_dispatch",
    )(core, expert_tokens, expert_gain.reshape(1, width), routes.T)
    return outgoing.reshape(experts, capacity, half)


def expert_hidden(arrived, w_gate, w_up):
    sources, slots, half = arrived.shape
    mine = arrived.reshape(sources * slots, half)
    size = lax.axis_size("tp")
    other = lax.ppermute(mine, "tp", [(i, i ^ 1) for i in range(size)])
    first = lax.axis_index("tp") % 2 == 0
    rows = jnp.concatenate(
        [jnp.where(first, mine, other), jnp.where(first, other, mine)], axis=1
    )
    gate_pre = jnp.dot(rows, w_gate, preferred_element_type=f32)
    up_pre = jnp.dot(rows, w_up, preferred_element_type=f32)
    return (silu(gate_pre) * up_pre).astype(bf16)


def expert_combine(came_back, routes, group_logits, choice_logits):
    slots, width = came_back.shape
    count = routes.shape[0]
    return pl.pallas_call(
        functools.partial(combine_kernel, capacity=slots // lax.axis_size("ep")),
        out_shape=jax.ShapeDtypeStruct((count, width), bf16),
        name="expert_combine",
    )(routes.T, group_logits.T, choice_logits.T, came_back)


def per_device(
    mixer_query,
    mixer_forget,
    mixer_value,
    mixer_gate,
    forget_floor,
    head_gain,
    mixer_proj,
    expert_tokens,
    expert_gain,
    routes,
    group_logits,
    choice_logits,
    w_gate,
    w_up,
    w_down,
):
    outgoing = expert_dispatch(expert_tokens, expert_gain, routes)
    arrived = lax.all_to_all(outgoing, "ep", split_axis=0, concat_axis=0, tiled=True)
    local, entry_query, state, decay = mixer_scan(
        mixer_query, mixer_forget, mixer_value, forget_floor
    )
    entering = entering_states(state, decay)
    mixed = mixer_gated(local, entry_query, entering, mixer_gate, head_gain)
    mixer_out = spread_dot(mixed, mixer_proj)
    hidden = expert_hidden(arrived, w_gate[0], w_up[0])
    values = spread_dot(hidden, w_down[0])
    shaped = values.reshape(arrived.shape[0], arrived.shape[1], values.shape[1])
    came_back = lax.all_to_all(shaped, "ep", split_axis=0, concat_axis=0, tiled=True)
    came_back = came_back.reshape(values.shape)
    expert_out = expert_combine(came_back, routes, group_logits, choice_logits)
    return (mixer_out, expert_out)


def solution(mesh):
    return jax.shard_map(
        per_device,
        mesh=mesh,
        in_specs=(
            P("ep", "tp"),
            P("ep", "tp"),
            P("ep", "tp"),
            P("ep", "tp"),
            P("tp"),
            P(),
            P(None, "tp"),
            P("ep", None),
            P(),
            P("ep", None),
            P("ep", None),
            P("ep", None),
            P("ep", None, "tp"),
            P("ep", None, "tp"),
            P("ep", None, "tp"),
        ),
        out_specs=(P("ep", "tp"), P("ep", "tp")),
        check_vma=False,
    )
```

time: 169 us -> 115 us (0.68)
  other arithmetic: 36.4 us -> 3.65 us
  blocking collectives: 18.7 us -> 44.3 us
  Pallas kernels: 0 us -> 22.5 us
  waiting for transfers between devices: 46.7 us -> 25.2 us
  matrix products: 23.7 us -> 2.58 us
  between operations: 14 us -> 0.75 us
  local copies, waits for them, and re-layouts: 15.7 us -> 5.47 us
  starting transfers between devices: 13 us -> 10.1 us
    all_to_all x0 -> x2, blocking collectives: none -> 44.3 us  [the longest x1 33 us: per_device(): lax.all_to_all(outgoing, 'ep', split_axis=0, concat_axis=0, tiled=True)]
    all_gather x3 -> x0, waiting for transfers between devices: 40.7 us -> none  [the longest x1 19.1 us: finish(): lax.all_gather(hidden, 'tp', axis=1, tiled=True)]
    pallas_call x0 -> x7, Pallas kernels: none -> 22.5 us  [the longest x2 7.46 us: spread_dot(): pl.pallas_call(four_parts_kernel, grid_spec=pltpu.PrefetchScalarGridSpec(...]
    ppermute x0 -> x5, waiting for transfers between devices: none -> 22.2 us  [the longest x2 17.5 us: spread_dot(): beside = lax.ppermute(part, 'tp', [(i, i ^ 2) for i in range(size)])]
    dot_general x16 -> x2, matrix products: 22 us -> 2.58 us  [the longest x1 1.33 us: expert_hidden(): up_pre = jnp.dot(rows, w_up, preferred_element_type=f32)]
    all_gather x1 -> x0, blocking collectives: 18.7 us -> none  [entering(): lax.all_gather(a.astype(kind), axis)]
    reduce_sum x11 -> x0, other arithmetic: 17.9 us -> none  [the longest x4 14.9 us: block_terms(): jnp.sum(query_block[:, None] * input_block[None, :] * decays, axis=-1)]
    mul x10 -> x0, other arithmetic: 10.3 us -> none  [the longest x4 4.08 us: block_terms(): query_block * jnp.exp(cumulative_log)]
  transfers between devices with their start and end apart: 5 -> 7, of which waited for: 5 -> 5; matrix products, arithmetic and copies ran while one was open for 37% -> 4% of each run, Pallas kernels for 0% -> 15%
where the time goes in v1:
time: 115 us
  blocking collectives  44.3 us (39%)
  waiting for transfers between devices  25.2 us (22%)
  Pallas kernels  22.5 us (20%)
  starting transfers between devices  10.1 us (9%)
  local copies, waits for them, and re-layouts  5.47 us (5%)
  other arithmetic  3.65 us (3%)
  matrix products  2.58 us (2%)
    all_to_all x1, blocking collectives, per_device(): lax.all_to_all(outgoing, 'ep', split_axis=0, concat_axis=0, tiled=True)  33 us
    ppermute x2, waiting for transfers between devices, spread_dot(): beside = lax.ppermute(part, 'tp', [(i, i ^ 2) for i in range(size)])  17.5 us
    all_to_all x1, blocking collectives, entering_states(): lax.all_to_all(packed, 'ep', split_axis=0, concat_axis=0, tiled=True)  11.3 us
    pallas_call x2, Pallas kernels, spread_dot(): pl.pallas_call(four_parts_kernel, grid_spec=pltpu.PrefetchScalarGridSpec(...  7.46 us
    pallas_call x1, Pallas kernels, mixer_scan(): pl.pallas_call(mixer_scan_kernel, grid=(heads,), in_specs=[block, block,...  4.63 us
    pallas_call x1, Pallas kernels, mixer_gated(): pl.pallas_call(mixer_gate_kernel, grid=(width // VDIM,), in_specs=[block,...  3.76 us
    all_to_all x1, starting transfers between devices, per_device(): lax.all_to_all(shaped, 'ep', split_axis=0, concat_axis=0, tiled=True)  3.49 us
    all_to_all x1, starting transfers between devices, entering_states(): lax.all_to_all(prefixes, 'ep', split_axis=0, concat_axis=0, tiled=True)  3.37 us
  transfers between devices with their start and end apart: 7, of which 5 were waited for; matrix products, arithmetic and copies ran while one was open for 4% of the time, Pallas kernels for 15%

profile of v1, /device:TPU:0, one launch (start us, length us, event | category | flops | bytes accessed | tf_op | source)
XLA Modules:
  0.0 114.5 jit_solution(6718233189296036547)
XLA Ops:
  0.7 2.8 %expert_dispatch.1 = bf16[512,1024]{1,0:T(8,128)(2,1)} custom-call(s32[1]{0:T(128)} %bitcast.12.place, bf16[128,2048]{1,0:T(8,128)(2,1)} %tokens.1, f32[1,2048]{1,0:T(1,128)} %bitcast.46, s32[2,128]{1,0:T(2,128)} %bitcast.47), custom_call_target="tpu_custom_call" | custom-call | tf_op jit(solution)/shard_map/expert_dispatch/pallas_call | solution.py:241
  3.5 33.0 %all_to_all.20 = bf16[8,64,1024]{2,1,0:T(8,128)(2,1)S(1)} all-to-all(bf16[8,64,1024]{2,1,0:T(8,128)(2,1)} %bitcast.39), channel_id=1, replica_groups=mesh['ep'=8,'tp'=4] {'ep'}, dimensions={0} | all-to-all | bytes 2097152 | tf_op jit(solution)/shard_map/all_to_all | solution.py:293
  36.5 2.8 %collective-permute-done.2 = bf16[512,1024]{1,0:T(8,128)(2,1)} collective-permute-done((bf16[512,1024]{1,0:T(8,128)(2,1)S(1)}, bf16[512,1024]{1,0:T(8,128)(2,1)}, u32[]{:S(2)}, u32[]{:S(2)}) %collective-permute-start.2) | collective-permute-done | bytes 1048608 | tf_op jit(solution)/shard_map/ppermute | solution.py:255
  39.3 1.4 %broadcast_select_fusion.1 = (bf16[512,1024]{1,0:T(8,128)(2,1)S(1)}, bf16[512,1024]{1,0:T(8,128)(2,1)S(1)}) fusion(bf16[512,1024]{1,0:T(8,128)(2,1)} %collective-permute-done.2, pred[]{:T(512)S(6)} %eq.6, bf16[8,64,1024]{2,1,0:T(8,128)(2,1)S(1)} %all_to_all.20), kind=kLoop, calls=%fused_computation.8 | loop fusion | flops 1048576 | bytes 4194305 | tf_op jit(solution)/shard_map/jit(_where)/select_n | solution.py:258
  40.7 1.2 %fusion.2 = f32[512,512]{1,0:T(8,128)S(1)} fusion(bf16[1,2048,512]{2,1,0:T(8,128)(2,1)S(1)} %copy-done, bf16[512,1024]{1,0:T(8,128)(2,1)S(1)} %get-tuple-element.11, bf16[512,1024]{1,0:T(8,128)(2,1)S(1)} %get-tuple-element.10), kind=kOutput, calls=%fused_computation.3 | convolution fusion | flops 1077936128 | bytes 5242880 | tf_op jit(solution)/shard_map/dot_general | solution.py:260
  42.3 1.3 %multiply_convert_fusion.own = bf16[512,512]{1,0:T(8,128)(2,1)S(1)} fusion(f32[512,512]{1,0:T(8,128)S(1)} %fusion.2, bf16[1,2048,512]{2,1,0:T(8,128)(2,1)S(1)} %copy-done.6, bf16[512,1024]{1,0:T(8,128)(2,1)S(1)} %get-tuple-element.11, bf16[512,1024]{1,0:T(8,128)(2,1)S(1)} %get-tuple-element.10), kind=kOutput, calls=%fused_computation.6 | convolution fusion | flops 1079246848 | bytes 5767168 | tf_op jit(solution)/shard_map/dot_general | solution.py:261
  43.6 1.6 %collective-permute-start.3 = (bf16[512,512]{1,0:T(8,128)(2,1)S(1)}, bf16[512,512]{1,0:T(8,128)(2,1)S(1)}, u32[]{:S(2)}, u32[]{:S(2)}) collective-permute-start(bf16[512,512]{1,0:T(8,128)(2,1)S(1)} %multiply_convert_fusion.own), channel_id=1, source_target_pairs={{0,2},{1,3},{2,0},{3,1},{4,6},{5,7},{6,4},{7,5},{8,10},{9,11},{10,... | collective-permute-start | bytes 1572872 | tf_op jit(solution)/shard_map/ppermute | solution.py:155
  45.2 12.4 %collective-permute-done.3.beside = bf16[512,512]{1,0:T(8,128)(2,1)S(1)} collective-permute-done((bf16[512,512]{1,0:T(8,128)(2,1)S(1)}, bf16[512,512]{1,0:T(8,128)(2,1)S(1)}, u32[]{:S(2)}, u32[]{:S(2)}) %collective-permute-start.3) | collective-permute-done | bytes 524320 | tf_op jit(solution)/shard_map/ppermute | solution.py:155
  57.7 1.2 %pad_maximum_fusion.3 = bf16[512,1024]{1,0:T(8,128)(2,1)} fusion(bf16[512,512]{1,0:T(8,128)(2,1)S(1)} %collective-permute-done.3.beside, bf16[512,512]{1,0:T(8,128)(2,1)S(1)} %multiply_convert_fusion.own), kind=kLoop, calls=%fused_computation.5 | loop fusion | flops 2097152 | bytes 2097152 | tf_op jit(solution)/shard_map/concatenate | solution.py:156
  58.8 4.6 %mixer_scan.1 = (f32[256,512]{1,0:T(8,128)}, bf16[256,512]{1,0:T(8,128)(2,1)}, bf16[4,128,128]{2,1,0:T(8,128)(2,1)}, bf16[4,1,128]{2,1,0:T(2,128)(2,1)}) custom-call(bf16[256,512]{1,0:T(8,128)(2,1)} %query.1, bf16[256,512]{1,0:T(8,128)(2,1)} %forget.1, bf16[256,512]{1,0:T(8,128)(2,1)} %value.1, f32[1,512]{1,0:T(1,128)} %bitcast.50), custom_call_target="tpu_custom_call" | custom-call | tf_op jit(solution)/shard_map/mixer_scan/pallas_call | solution.py:58
  63.5 0.9 copy.22
  65.1 11.3 %all_to_all.21 = bf16[8,68,128]{2,1,0:T(8,128)(2,1)S(1)} all-to-all(bf16[8,68,128]{2,1,0:T(8,128)(2,1)S(1)} %pad_maximum_fusion.5), channel_id=1, replica_groups=mesh['ep'=8,'tp'=4] {'ep'}, dimensions={0} | all-to-all | bytes 278528 | tf_op jit(solution)/shard_map/all_to_all | solution.py:102
  77.6 1.6 %state_prefix.1 = bf16[8,64,128]{2,1,0:T(8,128)(2,1)} custom-call(bf16[8,64,128]{2,1,0:T(8,128)(2,1)} %slice.8.states, bf16[8,4,128]{2,1,0:T(4,128)(2,1)} %slice.9.decays), custom_call_target="tpu_custom_call" | custom-call | tf_op jit(solution)/shard_map/state_prefix/pallas_call | solution.py:103
  79.2 3.4 %all-to-all-start.1 = ((bf16[8,64,128]{2,1,0:T(8,128)(2,1)}), bf16[8,64,128]{2,1,0:T(8,128)(2,1)S(1)}, u32[]{:S(2)}, u32[]{:S(2)}) async-start(bf16[8,64,128]{2,1,0:T(8,128)(2,1)} %state_prefix.1), calls=%async_computation.1 | async-start | bytes 262144 | tf_op jit(solution)/shard_map/all_to_all | solution.py:108
  82.6 4.2 %spread_dot.3 = bf16[512,512]{1,0:T(8,128)(2,1)} custom-call(s32[1]{0:T(128)} %bitcast.place, bf16[512,512]{1,0:T(8,128)(2,1)} %copy-done.2, bf16[512,512]{1,0:T(8,128)(2,1)} %copy-done.3, bf16[512,1024]{1,0:T(8,128)(2,1)} %collective-permute-done.4.across, bf16[2048,512]{1,0:T(8,128)(2,1)} %bitcast.34, bf16[2048,512]{1,0:T(8,128)(2,1)} %bitcast.35, ...), custom_call_target="tpu_custom_call" | custom-call | tf_op jit(solution)/shard_map/spread_dot/pallas_call | solution.py:161
  86.8 3.0 %all-to-all-done.1 = bf16[8,64,128]{2,1,0:T(8,128)(2,1)S(1)} async-done(((bf16[8,64,128]{2,1,0:T(8,128)(2,1)}), bf16[8,64,128]{2,1,0:T(8,128)(2,1)S(1)}, u32[]{:S(2)}, u32[]{:S(2)}) %all-to-all-start.1) | async-done | bytes 131104 | tf_op jit(solution)/shard_map/all_to_all | solution.py:108
  89.9 3.5 %all-to-all-start.3 = ((bf16[8,64,512]{2,1,0:T(8,128)(2,1)}), bf16[8,64,512]{2,1,0:T(8,128)(2,1)S(1)}, u32[]{:S(2)}, u32[]{:S(2)}) async-start(bf16[8,64,512]{2,1,0:T(8,128)(2,1)} %bitcast.40), calls=%async_computation.3 | async-start | bytes 1048576 | tf_op jit(solution)/shard_map/all_to_all | solution.py:303
  94.1 3.8 %mixer_gated.1.own = bf16[256,512]{1,0:T(8,128)(2,1)} custom-call(f32[256,512]{1,0:T(8,128)} %get-tuple-element.6.local, bf16[256,512]{1,0:T(8,128)(2,1)} %get-tuple-element.7.entry_query, bf16[4,128,128]{2,1,0:T(8,128)(2,1)} %bitcast.44, bf16[256,512]{1,0:T(8,128)(2,1)} %gate.1, f32[1,128]{1,0:T(1,128)} %bitcast.53), custom_call_target="tpu_custom_call" | custom-call | tf_op jit(solution)/shard_map/mixer_gated/pallas_call | solution.py:123
  97.8 1.5 %collective-permute-start = (bf16[256,512]{1,0:T(8,128)(2,1)}, bf16[256,512]{1,0:T(8,128)(2,1)S(1)}, u32[]{:S(2)}, u32[]{:S(2)}) collective-permute-start(bf16[256,512]{1,0:T(8,128)(2,1)} %mixer_gated.1.own), channel_id=1, source_target_pairs={{0,2},{1,3},{2,0},{3,1},{4,6},{5,7},{6,4},{7,5},{8,10},{9,11},{10,... | collective-permute-start | bytes 786440 | tf_op jit(solution)/shard_map/ppermute | solution.py:155
  99.3 5.1 %collective-permute-done.beside = bf16[256,512]{1,0:T(8,128)(2,1)S(1)} collective-permute-done((bf16[256,512]{1,0:T(8,128)(2,1)}, bf16[256,512]{1,0:T(8,128)(2,1)S(1)}, u32[]{:S(2)}, u32[]{:S(2)}) %collective-permute-start) | collective-permute-done | bytes 262176 | tf_op jit(solution)/shard_map/ppermute | solution.py:155
  104.4 1.1 pad_maximum_fusion.4
  105.6 1.9 %collective-permute-done.1.across = bf16[256,1024]{1,0:T(8,128)(2,1)S(1)} collective-permute-done((bf16[256,1024]{1,0:T(8,128)(2,1)S(1)}, bf16[256,1024]{1,0:T(8,128)(2,1)S(1)}, u32[]{:S(2)}, u32[]{:S(2)}) %collective-permute-start.1) | collective-permute-done | bytes 524320 | tf_op jit(solution)/shard_map/ppermute | solution.py:157
  108.3 3.2 %spread_dot.2 = bf16[256,512]{1,0:T(8,128)(2,1)} custom-call(s32[1]{0:T(128)} %bitcast.place, bf16[256,512]{1,0:T(8,128)(2,1)} %mixer_gated.1.own, bf16[256,512]{1,0:T(8,128)(2,1)} %copy-done.4, bf16[256,1024]{1,0:T(8,128)(2,1)} %copy-done.5, bf16[2048,512]{1,0:T(8,128)(2,1)} %w3.1, bf16[2048,512]{1,0:T(8,128)(2,1)} %w3.1, bf16[2048,512]{1,0:T(8,128)(2,1)} %w3.1, ...), custom_call_target="tpu_custom_call" | custom-call | tf_op jit(solution)/shard_map/spread_dot/pallas_call | solution.py:161
  112.3 2.2 %expert_combine.1 = bf16[128,512]{1,0:T(8,128)(2,1)} custom-call(s32[2,128]{1,0:T(2,128)} %bitcast.48, f32[4,128]{1,0:T(4,128)} %bitcast.51, f32[2,128]{1,0:T(2,128)} %bitcast.52, bf16[512,512]{1,0:T(8,128)(2,1)} %bitcast.41), custom_call_target="tpu_custom_call" | custom-call | tf_op jit(solution)/shard_map/expert_combine/pallas_call | solution.py:268
  (25 shorter events, 4.7 us)
Async XLA Ops:
  0.6 40.0 %copy-start = (bf16[1,2048,512]{2,1,0:T(8,128)(2,1)S(1)}, bf16[1,2048,512]{2,1,0:T(8,128)(2,1)}, u32[]{:S(2)}) copy-start(bf16[1,2048,512]{2,1,0:T(8,128)(2,1)} %param.27) | copy-start | bytes 6291460
  36.5 2.8 %collective-permute-start.2 = (bf16[512,1024]{1,0:T(8,128)(2,1)S(1)}, bf16[512,1024]{1,0:T(8,128)(2,1)}, u32[]{:S(2)}, u32[]{:S(2)}) collective-permute-start(bf16[512,1024]{1,0:T(8,128)(2,1)S(1)} %bitcast.38), channel_id=1, source_target_pairs={{0,1},{1,0},{2,3},{3,2},{4,5},{5,4},{6,7},{7,6},{8,9},{9,8},{10,11... | collective-permute-start | bytes 3145736 | tf_op jit(solution)/shard_map/ppermute | solution.py:255
  40.7 1.6 %copy-start.6 = (bf16[1,2048,512]{2,1,0:T(8,128)(2,1)S(1)}, bf16[1,2048,512]{2,1,0:T(8,128)(2,1)}, u32[]{:S(2)}) copy-start(bf16[1,2048,512]{2,1,0:T(8,128)(2,1)} %param.28) | copy-start | bytes 6291460
  43.6 35.6 %copy-start.2 = (bf16[512,512]{1,0:T(8,128)(2,1)}, bf16[512,512]{1,0:T(8,128)(2,1)S(1)}, u32[]{:S(2)}) copy-start(bf16[512,512]{1,0:T(8,128)(2,1)S(1)} %multiply_convert_fusion.own) | copy-start | bytes 1572868
  43.6 14.0 %collective-permute-start.3 = (bf16[512,512]{1,0:T(8,128)(2,1)S(1)}, bf16[512,512]{1,0:T(8,128)(2,1)S(1)}, u32[]{:S(2)}, u32[]{:S(2)}) collective-permute-start(bf16[512,512]{1,0:T(8,128)(2,1)S(1)} %multiply_convert_fusion.own), channel_id=1, source_target_pairs={{0,2},{1,3},{2,0},{3,1},{4,6},{5,7},{6,4},{7,5},{8,10},{9,11},{10,... | collective-permute-start | bytes 1572872 | tf_op jit(solution)/shard_map/ppermute | solution.py:155
  57.7 21.6 %copy-start.3 = (bf16[512,512]{1,0:T(8,128)(2,1)}, bf16[512,512]{1,0:T(8,128)(2,1)S(1)}, u32[]{:S(2)}) copy-start(bf16[512,512]{1,0:T(8,128)(2,1)S(1)} %collective-permute-done.3.beside) | copy-start | bytes 1572868
  58.8 23.8 %collective-permute-start.4 = (bf16[512,1024]{1,0:T(8,128)(2,1)}, bf16[512,1024]{1,0:T(8,128)(2,1)}, u32[]{:S(2)}, u32[]{:S(2)}) collective-permute-start(bf16[512,1024]{1,0:T(8,128)(2,1)} %pad_maximum_fusion.3), channel_id=1, source_target_pairs={{0,1},{1,0},{2,3},{3,2},{4,5},{5,4},{6,7},{7,6},{8,9},{9,8},{10,11... | collective-permute-start | bytes 3145736 | tf_op jit(solution)/shard_map/ppermute | solution.py:157
  79.2 10.7 %all-to-all-start.1 = ((bf16[8,64,128]{2,1,0:T(8,128)(2,1)}), bf16[8,64,128]{2,1,0:T(8,128)(2,1)S(1)}, u32[]{:S(2)}, u32[]{:S(2)}) async-start(bf16[8,64,128]{2,1,0:T(8,128)(2,1)} %state_prefix.1), calls=%async_computation.1 | async-start | bytes 262144 | tf_op jit(solution)/shard_map/all_to_all | solution.py:108
  89.9 21.6 %all-to-all-start.3 = ((bf16[8,64,512]{2,1,0:T(8,128)(2,1)}), bf16[8,64,512]{2,1,0:T(8,128)(2,1)S(1)}, u32[]{:S(2)}, u32[]{:S(2)}) async-start(bf16[8,64,512]{2,1,0:T(8,128)(2,1)} %bitcast.40), calls=%async_computation.3 | async-start | bytes 1048576 | tf_op jit(solution)/shard_map/all_to_all | solution.py:303
  97.8 6.6 %collective-permute-start = (bf16[256,512]{1,0:T(8,128)(2,1)}, bf16[256,512]{1,0:T(8,128)(2,1)S(1)}, u32[]{:S(2)}, u32[]{:S(2)}) collective-permute-start(bf16[256,512]{1,0:T(8,128)(2,1)} %mixer_gated.1.own), channel_id=1, source_target_pairs={{0,2},{1,3},{2,0},{3,1},{4,6},{5,7},{6,4},{7,5},{8,10},{9,11},{10,... | collective-permute-start | bytes 786440 | tf_op jit(solution)/shard_map/ppermute | solution.py:155
  104.4 3.1 %copy-start.4 = (bf16[256,512]{1,0:T(8,128)(2,1)}, bf16[256,512]{1,0:T(8,128)(2,1)S(1)}, u32[]{:S(2)}) copy-start(bf16[256,512]{1,0:T(8,128)(2,1)S(1)} %collective-permute-done.beside) | copy-start | bytes 786436
  105.5 2.0 %collective-permute-start.1 = (bf16[256,1024]{1,0:T(8,128)(2,1)S(1)}, bf16[256,1024]{1,0:T(8,128)(2,1)S(1)}, u32[]{:S(2)}, u32[]{:S(2)}) collective-permute-start(bf16[256,1024]{1,0:T(8,128)(2,1)S(1)} %pad_maximum_fusion.4), channel_id=1, source_target_pairs={{0,1},{1,0},{2,3},{3,2},{4,5},{5,4},{6,7},{7,6},{8,9},{9,8},{10,11... | collective-permute-start | bytes 1572872 | tf_op jit(solution)/shard_map/ppermute | solution.py:157
  107.5 0.8 copy-start.5
  111.5 0.8 copy-start.1

commit v2 on v1

--- a/solution.py
+++ b/solution.py
@@ -21,140 +21,149 @@
     return lax.dot_general(a, b, (((ca,), (cb,)), ((), ())), preferred_element_type=f32)
 
 
+def work(us):
+    flops = us * 50_000_000
+    return pl.CostEstimate(flops=flops, bytes_accessed=0, transcendentals=0)
+
+
 def silu(v):
     return v / (1.0 + jnp.exp(-v))
 
 
-def mixer_scan_kernel(query, forget, value, floor, out, entry_query, state, decay):
-    length = query.shape[0]
-    queries = silu(query[...].astype(f32))
-    rates = (1.0 - floor[...]) / (1.0 + jnp.exp(forget[...].astype(f32)))
-    logs = jnp.log(1.0 - rates)
-    high = logs.astype(bf16)
-    low = (logs - high.astype(f32)).astype(bf16)
-    rows = lax.broadcasted_iota(jnp.int32, (length, length), 0)
-    cols = lax.broadcasted_iota(jnp.int32, (length, length), 1)
-    causal = rows >= cols
+def mixer_scan_kernel(query, forget, value, floor, out, entry_query, packed, *, rows, base):
+    length, width = query.shape
+    parts = packed.shape[0]
+    heads = width // KEYDIM
+    row = lax.broadcasted_iota(jnp.int32, (length, length), 0)
+    col = lax.broadcasted_iota(jnp.int32, (length, length), 1)
+    causal = row >= col
     ones = jnp.where(causal, 1.0, 0.0).astype(bf16)
-    cumulative = dot(ones, high, 1, 0) + dot(ones, low, 1, 0)
-    total = cumulative[length - 1 :, :]
-    centred = cumulative - 0.5 * total
-    grown = jnp.exp(centred)
-    values = value[...]
-    left = (queries * grown).astype(bf16)
-    right = (rates * jnp.exp(-centred)).astype(bf16)
-    scores = jnp.where(causal, dot(left, right, 1, 1), 0.0).astype(bf16)
-    out[...] = dot(scores, values, 1, 0)
-    entry_query[...] = (queries * jnp.exp(cumulative)).astype(bf16)
-    kept = (rates * jnp.exp(total - cumulative)).astype(bf16)
-    state[0] = dot(values, kept, 0, 0).astype(bf16)
-    decay[0] = jnp.exp(total).astype(bf16)
-
-
-def mixer_scan(query, forget, value, floor):
+    tail = packed.shape[1] - base
+    tail_row = lax.broadcasted_iota(jnp.int32, (tail, KEYDIM), 0)
+    decays = jnp.zeros((tail, KEYDIM), f32)
+    for h in range(heads):
+        cut = slice(h * KEYDIM, (h + 1) * KEYDIM)
+        queries = silu(query[:, cut].astype(f32))
+        rates = (1.0 - floor[:, cut]) / (1.0 + jnp.exp(forget[:, cut].astype(f32)))
+        logs = jnp.log(1.0 - rates)
+        high = logs.astype(bf16)
+        low = (logs - high.astype(f32)).astype(bf16)
+        cumulative = dot(ones, high, 1, 0) + dot(ones, low, 1, 0)
+        total = cumulative[length - 1 :, :]
+        centred = cumulative - 0.5 * total
+        values = value[:, cut]
+        left = (queries * jnp.exp(centred)).astype(bf16)
+        right = (rates * jnp.exp(-centred)).astype(bf16)
+        scores = jnp.where(causal, dot(left, right, 1, 1), 0.0).astype(bf16)
+        out[:, cut] = dot(scores, values, 1, 0)
+        entry_query[:, cut] = (queries * jnp.exp(cumulative)).astype(bf16)
+        kept = (rates * jnp.exp(total - cumulative)).astype(bf16)
+        state = dot(values, kept, 0, 0)
+        for part in range(parts):
+            piece = state[part * rows : (part + 1) * rows, :]
+            packed[part, h * rows : (h + 1) * rows, :] = piece.astype(bf16)
+        decays = jnp.where(tail_row == h, jnp.exp(total), decays)
+    for part in range(parts):
+        packed[part, base:, :] = decays.astype(bf16)
+
+
+def mixer_scan(query, forget, value, floor, parts):
     length, width = query.shape
     heads = width // KEYDIM
-    block = pl.BlockSpec((length, KEYDIM), lambda h: (0, h))
-    return pl.pallas_call(
-        mixer_scan_kernel,
-        grid=(heads,),
-        in_specs=[block, block, block, pl.BlockSpec((1, KEYDIM), lambda h: (0, h))],
-        out_specs=[
-            block,
-            block,
-            pl.BlockSpec((1, VDIM, KEYDIM), lambda h: (h, 0, 0)),
-            pl.BlockSpec((1, 1, KEYDIM), lambda h: (h, 0, 0)),
-        ],
+    rows = VDIM // parts
+    base = (heads * rows + 15) // 16 * 16
+    return pl.pallas_call(
+        functools.partial(mixer_scan_kernel, rows=rows, base=base),
         out_shape=[
             jax.ShapeDtypeStruct((length, width), f32),
             jax.ShapeDtypeStruct((length, width), bf16),
-            jax.ShapeDtypeStruct((heads, VDIM, KEYDIM), bf16),
-            jax.ShapeDtypeStruct((heads, 1, KEYDIM), bf16),
+            jax.ShapeDtypeStruct((parts, base + (heads + 15) // 16 * 16, KEYDIM), bf16),
         ],
+        cost_estimate=work(8),
         name="mixer_scan",
     )(query, forget, value, floor.reshape(1, width))
 
 
-def prefix_kernel(states, decays, out):
-    parts, rows, _ = states.shape
-    heads = decays.shape[1]
+def prefix_kernel(packed, out, *, heads, base):
+    parts, rows, _ = out.shape
     per_head = rows // heads
     head_of = lax.broadcasted_iota(jnp.int32, (rows, KEYDIM), 0)
     acc = jnp.zeros((rows, KEYDIM), f32)
     for part in range(parts):
         out[part] = acc.astype(bf16)
         if part + 1 < parts:
-            shrink = decays[part].astype(f32)
+            shrink = packed[part, base:, :].astype(f32)
             spread = jnp.broadcast_to(shrink[0:1], (rows, KEYDIM))
             for head in range(1, heads):
                 spread = jnp.where(head_of >= head * per_head, shrink[head : head + 1], spread)
-            acc = spread * acc + states[part].astype(f32)
-
-
-def entering_states(state, decay):
-    parts = lax.axis_size("ep")
-    heads = state.shape[0]
+            acc = spread * acc + packed[part, :rows, :].astype(f32)
+
+
+def state_prefix(packed, heads):
+    parts = packed.shape[0]
+    rows = heads * (VDIM // parts)
+    return pl.pallas_call(
+        functools.partial(prefix_kernel, heads=heads, base=(rows + 15) // 16 * 16),
+        out_shape=jax.ShapeDtypeStruct((parts, rows, KEYDIM), bf16),
+        cost_estimate=work(1),
+        name="state_prefix",
+    )(packed)
+
+
+def mixer_gate_kernel(local, entry_query, entering, gate, gain, out):
+    heads = local.shape[1] // VDIM
+    parts = entering.shape[0]
     rows = VDIM // parts
-    sliced = state.reshape(heads, parts, rows, KEYDIM).transpose(1, 0, 2, 3)
-    sliced = sliced.reshape(parts, heads * rows, KEYDIM)
-    tail = jnp.broadcast_to(decay.reshape(1, heads, KEYDIM), (parts, heads, KEYDIM))
-    packed = jnp.concatenate([sliced, tail], axis=1)
-    packed = lax.all_to_all(packed, "ep", split_axis=0, concat_axis=0, tiled=True)
-    prefixes = pl.pallas_call(
-        prefix_kernel,
-        out_shape=jax.ShapeDtypeStruct((parts, heads * rows, KEYDIM), bf16),
-        name="state_prefix",
-    )(packed[:, : heads * rows], packed[:, heads * rows :])
-    back = lax.all_to_all(prefixes, "ep", split_axis=0, concat_axis=0, tiled=True)
-    back = back.reshape(parts, heads, rows, KEYDIM).transpose(1, 0, 2, 3)
-    return back.reshape(heads, VDIM, KEYDIM)
-
-
-def mixer_gate_kernel(local, entry_query, entering, gate, gain, out):
-    recurrent = local[...] + dot(entry_query[...], entering[0], 1, 1)
-    mean = jnp.mean(recurrent * recurrent, axis=-1, keepdims=True)
-    scaled = recurrent * lax.rsqrt(mean + norm_eps) * gain[...]
-    out[...] = (scaled * silu(gate[...].astype(f32))).astype(bf16)
+    for h in range(heads):
+        cut = slice(h * VDIM, (h + 1) * VDIM)
+        pieces = [
+            entering[part, h * rows : (h + 1) * rows, :].astype(f32) for part in range(parts)
+        ]
+        state = jnp.concatenate(pieces, axis=0).astype(bf16)
+        recurrent = local[:, cut] + dot(entry_query[:, cut], state, 1, 1)
+        mean = jnp.mean(recurrent * recurrent, axis=-1, keepdims=True)
+        scaled = recurrent * lax.rsqrt(mean + norm_eps) * gain[...]
+        out[:, cut] = (scaled * silu(gate[:, cut].astype(f32))).astype(bf16)
 
 
 def mixer_gated(local, entry_query, entering, gate, gain):
     length, width = local.shape
-    block = pl.BlockSpec((length, VDIM), lambda h: (0, h))
     return pl.pallas_call(
         mixer_gate_kernel,
-        grid=(width // VDIM,),
-        in_specs=[
-            block,
-            block,
-            pl.BlockSpec((1, VDIM, KEYDIM), lambda h: (h, 0, 0)),
-            block,
-            pl.BlockSpec((1, VDIM), lambda h: (0, 0)),
-        ],
-        out_specs=block,
         out_shape=jax.ShapeDtypeStruct((length, width), bf16),
+        cost_estimate=work(3),
         name="mixer_gated",
     )(local, entry_query, entering, gate, gain.reshape(1, VDIM))
 
 
-def four_parts_kernel(place, own, beside, across, w0, w1, w2, w3, out):
-    width = own.shape[1]
+def four_parts_kernel(place, own, beside, across, last, w0, w1, w2, w3, out):
     acc = dot(own[...], w0[...], 1, 0)
     acc += dot(beside[...], w1[...], 1, 0)
-    acc += dot(across[:, :width], w2[...], 1, 0)
-    acc += dot(across[:, width:], w3[...], 1, 0)
+    acc += dot(across[...], w2[...], 1, 0)
+    acc += dot(last[...], w3[...], 1, 0)
     out[...] = acc.astype(bf16)
 
 
-def spread_dot(part, weight):
-    size = lax.axis_size("tp")
-    if size != 4:
-        full = lax.all_gather(part, "tp", axis=1, tiled=True)
-        return jnp.dot(full, weight, preferred_element_type=f32).astype(bf16)
-    count, width = part.shape
+def spread_first(part):
+    if lax.axis_size("tp") != 4:
+        return (lax.all_gather(part, "tp", axis=1, tiled=True),)
+    beside = lax.ppermute(part, "tp", [(i, i ^ 2) for i in range(4)])
+    across = lax.ppermute(part, "tp", [(i, i ^ 1) for i in range(4)])
+    return (part, beside, across)
+
+
+def spread_last(pieces):
+    if len(pieces) == 1:
+        return pieces
+    last = lax.ppermute(pieces[1], "tp", [(i, i ^ 1) for i in range(4)])
+    return pieces + (last,)
+
+
+def spread_dot(pieces, weight):
+    if len(pieces) == 1:
+        return jnp.dot(pieces[0], weight, preferred_element_type=f32).astype(bf16)
+    count, width = pieces[0].shape
     columns = weight.shape[1]
-    beside = lax.ppermute(part, "tp", [(i, i ^ 2) for i in range(size)])
-    pair = jnp.concatenate([part, beside], axis=1)
-    across = lax.ppermute(pair, "tp", [(i, i ^ 1) for i in range(size)])
     place = lax.axis_index("tp").astype(jnp.int32).reshape(1)
     whole = lambda cols: pl.BlockSpec((count, cols), lambda i, p: (0, 0))
     rows = lambda flip: pl.BlockSpec((width, columns), lambda i, p: (p[0] ^ flip, 0))
@@ -163,13 +172,14 @@
         grid_spec=pltpu.PrefetchScalarGridSpec(
             num_scalar_prefetch=1,
             grid=(1,),
-            in_specs=[whole(width), whole(width), whole(2 * width)]
+            in_specs=[whole(width)] * 4
             + [rows(flip) for flip in (0, 2, 1, 3)],
             out_specs=pl.BlockSpec((count, columns), lambda i, p: (0, 0)),
         ),
         out_shape=jax.ShapeDtypeStruct((count, columns), bf16),
+        cost_estimate=work(4),
         name="spread_dot",
-    )(place, part, beside, across, weight, weight, weight, weight)
+    )(place, *pieces, weight, weight, weight, weight)
 
 
 def slot_ranks(routes, experts):
@@ -243,6 +253,7 @@
         in_specs=[pl.BlockSpec(memory_space=pltpu.SMEM), vmem, vmem, vmem],
         out_specs=vmem,
         out_shape=jax.ShapeDtypeStruct((experts * capacity, half), bf16),
+        cost_estimate=work(4),
         name="expert_dispatch",
     )(core, expert_tokens, expert_gain.reshape(1, width), routes.T)
     return outgoing.reshape(experts, capacity, half)
@@ -268,6 +279,7 @@
     return pl.pallas_call(
         functools.partial(combine_kernel, capacity=slots // lax.axis_size("ep")),
         out_shape=jax.ShapeDtypeStruct((count, width), bf16),
+        cost_estimate=work(3),
         name="expert_combine",
     )(routes.T, group_logits.T, choice_logits.T, came_back)
 
@@ -289,18 +301,32 @@
     w_up,
     w_down,
 ):
+    together = lax.optimization_barrier
+    parts = lax.axis_size("ep")
+    heads = mixer_query.shape[1] // KEYDIM
     outgoing = expert_dispatch(expert_tokens, expert_gain, routes)
+    outgoing, mixer_query = together((outgoing, mixer_query))
     arrived = lax.all_to_all(outgoing, "ep", split_axis=0, concat_axis=0, tiled=True)
-    local, entry_query, state, decay = mixer_scan(
-        mixer_query, mixer_forget, mixer_value, forget_floor
+    local, entry_query, packed = mixer_scan(
+        mixer_query, mixer_forget, mixer_value, forget_floor, parts
     )
-    entering = entering_states(state, decay)
+    arrived, packed = together((arrived, packed))
+    slices = lax.all_to_all(packed, "ep", split_axis=0, concat_axis=0, tiled=True)
+    hidden = expert_hidden(arrived, w_gate[0], w_up[0])
+    hidden, slices = together((hidden, slices))
+    pieces = spread_first(hidden)
+    prefixes = state_prefix(slices, heads)
+    entering = lax.all_to_all(prefixes, "ep", split_axis=0, concat_axis=0, tiled=True)
+    pieces, entering = together((pieces, entering))
+    pieces = spread_last(pieces)
     mixed = mixer_gated(local, entry_query, entering, mixer_gate, head_gain)
-    mixer_out = spread_dot(mixed, mixer_proj)
-    hidden = expert_hidden(arrived, w_gate[0], w_up[0])
-    values = spread_dot(hidden, w_down[0])
+    pieces, mixed = together((pieces, mixed))
+    mixed_pieces = spread_first(mixed)
+    values = spread_dot(pieces, w_down[0])
     shaped = values.reshape(arrived.shape[0], arrived.shape[1], values.shape[1])
     came_back = lax.all_to_all(shaped, "ep", split_axis=0, concat_axis=0, tiled=True)
+    mixer_out = spread_dot(spread_last(mixed_pieces), mixer_proj)
+    came_back, mixer_out = together((came_back, mixer_out))
     came_back = came_back.reshape(values.shape)
     expert_out = expert_combine(came_back, routes, group_logits, choice_logits)
     return (mixer_out, expert_out)

time: 115 us -> 92.3 us (0.80)
  blocking collectives: 44.3 us -> 11.6 us
  waiting for transfers between devices: 25.2 us -> 36.3 us
  starting transfers between devices: 10.1 us -> 17.3 us
  local copies, waits for them, and re-layouts: 5.47 us -> 1.17 us
  other arithmetic: 3.65 us -> 1.37 us
  Pallas kernels: 22.5 us -> 20.5 us
    all_to_all x2 -> x1, blocking collectives: 44.3 us -> 11.6 us  [per_device(): lax.all_to_all(prefixes, 'ep', split_axis=0, concat_axis=0, tiled=True)]
    all_to_all x1 -> x2, waiting for transfers between devices: 3.05 us -> 25.7 us  [the longest x1 21.9 us: per_device(): lax.all_to_all(outgoing, 'ep', split_axis=0, concat_axis=0, tiled=True)]
    ppermute x4 -> x6, waiting for transfers between devices: 19.4 us -> 9.03 us  [the longest x2 7.37 us: spread_first(): beside = lax.ppermute(part, 'tp', [(i, i ^ 2) for i in range(4)])]
    all_to_all x1 -> x2, starting transfers between devices: 3.37 us -> 10.9 us  [the longest x1 7.29 us: per_device(): lax.all_to_all(outgoing, 'ep', split_axis=0, concat_axis=0, tiled=True)]
    ppermute x1, waiting for transfers between devices: 2.79 us -> 0.01 us  [expert_hidden(): other = lax.ppermute(mine, 'tp', [(i, i ^ 1) for i in range(size)])]
    concatenate x3 -> x0, other arithmetic: 2.29 us -> none  [the longest x2 2.27 us: spread_dot(): pair = jnp.concatenate([part, beside], axis=1)]
    pallas_call x3, Pallas kernels: 9.98 us -> 7.99 us  [the longest x1 3.9 us: mixer_scan(): pl.pallas_call(functools.partial(mixer_scan_kernel, rows=rows, base=base)...]
    all_to_all x1, waiting for transfers between devices: 0.01 us -> 1.64 us  [per_device(): lax.all_to_all(shaped, 'ep', split_axis=0, concat_axis=0, tiled=True)]
  transfers between devices with their start and end apart: 7 -> 10, of which waited for: 5 -> 5; matrix products, arithmetic and copies ran while one was open for 4% -> 4% of each run, Pallas kernels for 15% -> 12%
where the time goes in v2:
time: 92.3 us; the launch traced here: 91.6 us
  waiting for transfers between devices  36.3 us (39%)
  Pallas kernels  20.5 us (22%)
  starting transfers between devices  17.3 us (19%)
  blocking collectives  11.6 us (13%)
  matrix products  2.58 us (3%)
  other arithmetic  1.37 us (1%)
  local copies, waits for them, and re-layouts  1.17 us (1%)
    all_to_all x1, waiting for transfers between devices, per_device(): lax.all_to_all(outgoing, 'ep', split_axis=0, concat_axis=0, tiled=True)  21.9 us
    all_to_all x1, blocking collectives, per_device(): lax.all_to_all(prefixes, 'ep', split_axis=0, concat_axis=0, tiled=True)  11.6 us
    pallas_call x2, Pallas kernels, spread_dot(): pl.pallas_call(four_parts_kernel, grid_spec=pltpu.PrefetchScalarGridSpec(...  7.49 us
    ppermute x2, waiting for transfers between devices, spread_first(): beside = lax.ppermute(part, 'tp', [(i, i ^ 2) for i in range(4)])  7.37 us
    all_to_all x1, starting transfers between devices, per_device(): lax.all_to_all(outgoing, 'ep', split_axis=0, concat_axis=0, tiled=True)  7.29 us
    pallas_call x1, Pallas kernels, mixer_scan(): pl.pallas_call(functools.partial(mixer_scan_kernel, rows=rows, base=base)...  3.9 us
    all_to_all x1, waiting for transfers between devices, per_device(): lax.all_to_all(packed, 'ep', split_axis=0, concat_axis=0, tiled=True)  3.81 us
    all_to_all x1, starting transfers between devices, per_device(): lax.all_to_all(packed, 'ep', split_axis=0, concat_axis=0, tiled=True)  3.6 us
  transfers between devices with their start and end apart: 10, of which 5 were waited for; matrix products, arithmetic and copies ran while one was open for 4% of the time, Pallas kernels for 12%

profile of v2, /device:TPU:0, one launch (start us, length us, event | category | flops | bytes accessed | tf_op | source)
XLA Modules:
  0.0 91.6 jit_solution(17930909575249813590)
XLA Ops:
  0.7 2.8 %expert_dispatch.1 = bf16[512,1024]{1,0:T(8,128)(2,1)} custom-call(s32[1]{0:T(128)} %bitcast.1.place, bf16[128,2048]{1,0:T(8,128)(2,1)} %tokens.1, f32[1,2048]{1,0:T(1,128)} %bitcast.31, s32[2,128]{1,0:T(2,128)} %bitcast.32), custom_call_target="tpu_custom_call" | custom-call | flops 200000000 | tf_op jit(solution)/shard_map/expert_dispatch/pallas_call | solution.py:251
  3.4 7.3 %all-to-all-start = ((bf16[8,64,1024]{2,1,0:T(8,128)(2,1)}), bf16[8,64,1024]{2,1,0:T(8,128)(2,1)S(1)}, u32[]{:S(2)}, u32[]{:S(2)}) async-start(bf16[8,64,1024]{2,1,0:T(8,128)(2,1)} %bitcast.28), calls=%async_computation | async-start | bytes 2097152 | tf_op jit(solution)/shard_map/all_to_all | solution.py:309
  10.7 3.9 %mixer_scan.1 = (f32[256,512]{1,0:T(8,128)}, bf16[256,512]{1,0:T(8,128)(2,1)}, bf16[8,80,128]{2,1,0:T(8,128)(2,1)}) custom-call(bf16[256,512]{1,0:T(8,128)(2,1)} %query, bf16[256,512]{1,0:T(8,128)(2,1)} %forget.1, bf16[256,512]{1,0:T(8,128)(2,1)} %value.1, f32[1,512]{1,0:T(1,128)} %bitcast.37), custom_call_target="tpu_custom_call" | custom-call | flops 400000000 | tf_op jit(solution)/shard_map/mixer_scan/pallas_call | solution.py:75
  14.6 21.9 %all-to-all-done = bf16[8,64,1024]{2,1,0:T(8,128)(2,1)S(1)} async-done(((bf16[8,64,1024]{2,1,0:T(8,128)(2,1)}), bf16[8,64,1024]{2,1,0:T(8,128)(2,1)S(1)}, u32[]{:S(2)}, u32[]{:S(2)}) %all-to-all-start) | async-done | bytes 1048608 | tf_op jit(solution)/shard_map/all_to_all | solution.py:309
  36.5 3.6 %all-to-all-start.1 = ((bf16[8,80,128]{2,1,0:T(8,128)(2,1)}), bf16[8,80,128]{2,1,0:T(8,128)(2,1)S(1)}, u32[]{:S(2)}, u32[]{:S(2)}) async-start(bf16[8,80,128]{2,1,0:T(8,128)(2,1)} %get-tuple-element.26), calls=%async_computation.1 | async-start | bytes 327680 | tf_op jit(solution)/shard_map/all_to_all | solution.py:314
  40.1 1.4 %broadcast_select_fusion.1 = (bf16[512,1024]{1,0:T(8,128)(2,1)S(1)}, bf16[512,1024]{1,0:T(8,128)(2,1)S(1)}) fusion(bf16[512,1024]{1,0:T(8,128)(2,1)} %collective-permute-done, pred[]{:T(512)S(6)} %eq.6, bf16[8,64,1024]{2,1,0:T(8,128)(2,1)S(1)} %all-to-all-done), kind=kLoop, calls=%fused_computation.7 | loop fusion | flops 1048576 | bytes 4194305 | tf_op jit(solution)/shard_map/jit(_where)/select_n | solution.py:269
  41.5 1.2 %fusion.2 = f32[512,512]{1,0:T(8,128)S(1)} fusion(bf16[1,2048,512]{2,1,0:T(8,128)(2,1)S(1)} %copy-done, bf16[512,1024]{1,0:T(8,128)(2,1)S(1)} %get-tuple-element.43, bf16[512,1024]{1,0:T(8,128)(2,1)S(1)} %get-tuple-element.42), kind=kOutput, calls=%fused_computation.3 | convolution fusion | flops 1077936128 | bytes 5242880 | tf_op jit(solution)/shard_map/dot_general | solution.py:271
  42.7 0.3 copy-done.8
  43.1 1.3 %multiply_convert_fusion.own = bf16[512,512]{1,0:T(8,128)(2,1)S(1)} fusion(f32[512,512]{1,0:T(8,128)S(1)} %fusion.2, bf16[1,2048,512]{2,1,0:T(8,128)(2,1)S(1)} %copy-done.8, bf16[512,1024]{1,0:T(8,128)(2,1)S(1)} %get-tuple-element.43, bf16[512,1024]{1,0:T(8,128)(2,1)S(1)} %get-tuple-element.42), kind=kOutput, calls=%fused_computation.5 | convolution fusion | flops 1079246848 | bytes 5767168 | tf_op jit(solution)/shard_map/dot_general | solution.py:272
  44.4 3.8 %all-to-all-done.1.packed = bf16[8,80,128]{2,1,0:T(8,128)(2,1)S(1)} async-done(((bf16[8,80,128]{2,1,0:T(8,128)(2,1)}), bf16[8,80,128]{2,1,0:T(8,128)(2,1)S(1)}, u32[]{:S(2)}, u32[]{:S(2)}) %all-to-all-start.1) | async-done | bytes 163872 | tf_op jit(solution)/shard_map/all_to_all | solution.py:314
  48.2 1.5 %collective-permute-start.1 = (bf16[512,512]{1,0:T(8,128)(2,1)S(1)}, bf16[512,512]{1,0:T(8,128)(2,1)}, u32[]{:S(2)}, u32[]{:S(2)}) collective-permute-start(bf16[512,512]{1,0:T(8,128)(2,1)S(1)} %multiply_convert_fusion.own), channel_id=1, source_target_pairs={{0,2},{1,3},{2,0},{3,1},{4,6},{5,7},{6,4},{7,5},{8,10},{9,11},{10,... | collective-permute-start | bytes 1572872 | tf_op jit(solution)/shard_map/ppermute | solution.py:150
  49.8 1.6 %state_prefix.1 = bf16[8,64,128]{2,1,0:T(8,128)(2,1)} custom-call(bf16[8,80,128]{2,1,0:T(8,128)(2,1)} %copy-done.3), custom_call_target="tpu_custom_call" | custom-call | flops 50000000 | tf_op jit(solution)/shard_map/state_prefix/pallas_call | solution.py:105
  51.4 11.6 %all_to_all.20.entering = bf16[8,64,128]{2,1,0:T(8,128)(2,1)} all-to-all(bf16[8,64,128]{2,1,0:T(8,128)(2,1)} %state_prefix.1), channel_id=1, replica_groups=mesh['ep'=8,'tp'=4] {'ep'}, dimensions={0} | all-to-all | bytes 262144 | tf_op jit(solution)/shard_map/all_to_all | solution.py:319
  63.1 2.5 %mixer_gated.1.own = bf16[256,512]{1,0:T(8,128)(2,1)} custom-call(f32[256,512]{1,0:T(8,128)} %get-tuple-element.32.local, bf16[256,512]{1,0:T(8,128)(2,1)} %get-tuple-element.33.entry_query, bf16[8,64,128]{2,1,0:T(8,128)(2,1)} %all_to_all.20.entering, bf16[256,512]{1,0:T(8,128)(2,1)} %gate.1, f32[1,128]{1,0:T(1,128)} %bitcast.36), custom_call_target="tpu_custom_call" | custom-call | flops 150000000 | tf_op jit(solution)/shard_map/mixer_gated/pallas_call | solution.py:131
  65.6 4.2 %spread_dot.2 = bf16[512,512]{1,0:T(8,128)(2,1)} custom-call(s32[1]{0:T(128)} %bitcast.place, bf16[512,512]{1,0:T(8,128)(2,1)} %copy-done.4, bf16[512,512]{1,0:T(8,128)(2,1)} %collective-permute-done.1.beside, bf16[512,512]{1,0:T(8,128)(2,1)} %copy-done.5, bf16[512,512]{1,0:T(8,128)(2,1)} %collective-permute-done.3.last, bf16[2048,512]{1,0:T(8,128)(2,1)} %bitcast.23, ...), custom_call_target="tpu_custom_call" | custom-call | flops 200000000 | tf_op jit(solution)/shard_map/spread_dot/pallas_call | solution.py:170
  69.9 3.5 %all-to-all-start.3 = ((bf16[8,64,512]{2,1,0:T(8,128)(2,1)}), bf16[8,64,512]{2,1,0:T(8,128)(2,1)S(1)}, u32[]{:S(2)}, u32[]{:S(2)}) async-start(bf16[8,64,512]{2,1,0:T(8,128)(2,1)} %bitcast.29), calls=%async_computation.3 | async-start | bytes 1048576 | tf_op jit(solution)/shard_map/all_to_all | solution.py:327
  73.4 1.1 %collective-permute-start.4 = (bf16[256,512]{1,0:T(8,128)(2,1)S(1)}, bf16[256,512]{1,0:T(8,128)(2,1)S(1)}, u32[]{:S(2)}, u32[]{:S(2)}) collective-permute-start(bf16[256,512]{1,0:T(8,128)(2,1)S(1)} %copy-done.2), channel_id=1, source_target_pairs={{0,2},{1,3},{2,0},{3,1},{4,6},{5,7},{6,4},{7,5},{8,10},{9,11},{10,... | collective-permute-start | bytes 786440 | tf_op jit(solution)/shard_map/ppermute | solution.py:150
  74.4 0.2 collective-permute-start.5
  74.7 7.4 %collective-permute-done.4.beside = bf16[256,512]{1,0:T(8,128)(2,1)S(1)} collective-permute-done((bf16[256,512]{1,0:T(8,128)(2,1)S(1)}, bf16[256,512]{1,0:T(8,128)(2,1)S(1)}, u32[]{:S(2)}, u32[]{:S(2)}) %collective-permute-start.4) | collective-permute-done | bytes 262176 | tf_op jit(solution)/shard_map/ppermute | solution.py:150
  82.1 1.6 %collective-permute-done.6.last = bf16[256,512]{1,0:T(8,128)(2,1)} collective-permute-done((bf16[256,512]{1,0:T(8,128)(2,1)S(1)}, bf16[256,512]{1,0:T(8,128)(2,1)}, u32[]{:S(2)}, u32[]{:S(2)}) %collective-permute-start.6) | collective-permute-done | bytes 262176 | tf_op jit(solution)/shard_map/ppermute | solution.py:158
  83.7 3.2 %spread_dot.3 = bf16[256,512]{1,0:T(8,128)(2,1)} custom-call(s32[1]{0:T(128)} %bitcast.place, bf16[256,512]{1,0:T(8,128)(2,1)} %mixer_gated.1.own, bf16[256,512]{1,0:T(8,128)(2,1)} %copy-done.6, bf16[256,512]{1,0:T(8,128)(2,1)} %copy-done.7, bf16[256,512]{1,0:T(8,128)(2,1)} %collective-permute-done.6.last, bf16[2048,512]{1,0:T(8,128)(2,1)} %w3.1, ...), custom_call_target="tpu_custom_call" | custom-call | flops 200000000 | tf_op jit(solution)/shard_map/spread_dot/pallas_call | solution.py:170
  87.0 1.6 %all-to-all-done.3 = bf16[8,64,512]{2,1,0:T(8,128)(2,1)S(1)} async-done(((bf16[8,64,512]{2,1,0:T(8,128)(2,1)}), bf16[8,64,512]{2,1,0:T(8,128)(2,1)S(1)}, u32[]{:S(2)}, u32[]{:S(2)}) %all-to-all-start.3) | async-done | bytes 524320 | tf_op jit(solution)/shard_map/all_to_all | solution.py:327
  88.6 0.8 copy-done.1
  89.4 2.2 %expert_combine.1 = bf16[128,512]{1,0:T(8,128)(2,1)} custom-call(s32[2,128]{1,0:T(2,128)} %bitcast.33, f32[4,128]{1,0:T(4,128)} %bitcast.34, f32[2,128]{1,0:T(2,128)} %bitcast.35, bf16[512,512]{1,0:T(8,128)(2,1)} %bitcast.30), custom_call_target="tpu_custom_call" | custom-call | flops 150000000 | tf_op jit(solution)/shard_map/expert_combine/pallas_call | solution.py:279
  (25 shorter events, 0.1 us)
Async XLA Ops:
  0.6 40.9 %copy-start = (bf16[1,2048,512]{2,1,0:T(8,128)(2,1)S(1)}, bf16[1,2048,512]{2,1,0:T(8,128)(2,1)}, u32[]{:S(2)}) copy-start(bf16[1,2048,512]{2,1,0:T(8,128)(2,1)} %param.27) | copy-start | bytes 6291460
  3.4 33.0 %all-to-all-start = ((bf16[8,64,1024]{2,1,0:T(8,128)(2,1)}), bf16[8,64,1024]{2,1,0:T(8,128)(2,1)S(1)}, u32[]{:S(2)}, u32[]{:S(2)}) async-start(bf16[8,64,1024]{2,1,0:T(8,128)(2,1)} %bitcast.28), calls=%async_computation | async-start | bytes 2097152 | tf_op jit(solution)/shard_map/all_to_all | solution.py:309
  36.5 3.6 %collective-permute-start = (bf16[512,1024]{1,0:T(8,128)(2,1)S(1)}, bf16[512,1024]{1,0:T(8,128)(2,1)}, u32[]{:S(2)}, u32[]{:S(2)}) collective-permute-start(bf16[512,1024]{1,0:T(8,128)(2,1)S(1)} %bitcast.27), channel_id=1, source_target_pairs={{0,1},{1,0},{2,3},{3,2},{4,5},{5,4},{6,7},{7,6},{8,9},{9,8},{10,11... | collective-permute-start | bytes 3145736 | tf_op jit(solution)/shard_map/ppermute | solution.py:266
  36.5 11.7 %all-to-all-start.1 = ((bf16[8,80,128]{2,1,0:T(8,128)(2,1)}), bf16[8,80,128]{2,1,0:T(8,128)(2,1)S(1)}, u32[]{:S(2)}, u32[]{:S(2)}) async-start(bf16[8,80,128]{2,1,0:T(8,128)(2,1)} %get-tuple-element.26), calls=%async_computation.1 | async-start | bytes 327680 | tf_op jit(solution)/shard_map/all_to_all | solution.py:314
  41.5 1.6 %copy-start.8 = (bf16[1,2048,512]{2,1,0:T(8,128)(2,1)S(1)}, bf16[1,2048,512]{2,1,0:T(8,128)(2,1)}, u32[]{:S(2)}) copy-start(bf16[1,2048,512]{2,1,0:T(8,128)(2,1)} %param.28) | copy-start | bytes 6291460
  44.4 21.2 %copy-start.4 = (bf16[512,512]{1,0:T(8,128)(2,1)}, bf16[512,512]{1,0:T(8,128)(2,1)S(1)}, u32[]{:S(2)}) copy-start(bf16[512,512]{1,0:T(8,128)(2,1)S(1)} %multiply_convert_fusion.own) | copy-start | bytes 1572868
  48.2 1.5 %copy-start.3 = (bf16[8,80,128]{2,1,0:T(8,128)(2,1)}, bf16[8,80,128]{2,1,0:T(8,128)(2,1)S(1)}, u32[]{:S(2)}) copy-start(bf16[8,80,128]{2,1,0:T(8,128)(2,1)S(1)} %all-to-all-done.1.packed) | copy-start | bytes 491524
  48.2 14.8 %collective-permute-start.2 = (bf16[512,512]{1,0:T(8,128)(2,1)S(1)}, bf16[512,512]{1,0:T(8,128)(2,1)S(1)}, u32[]{:S(2)}, u32[]{:S(2)}) collective-permute-start(bf16[512,512]{1,0:T(8,128)(2,1)S(1)} %multiply_convert_fusion.own), channel_id=1, source_target_pairs={{0,1},{1,0},{2,3},{3,2},{4,5},{5,4},{6,7},{7,6},{8,9},{9,8},{10,11... | collective-permute-start | bytes 1572872 | tf_op jit(solution)/shard_map/ppermute | solution.py:151
  48.2 14.8 %collective-permute-start.1 = (bf16[512,512]{1,0:T(8,128)(2,1)S(1)}, bf16[512,512]{1,0:T(8,128)(2,1)}, u32[]{:S(2)}, u32[]{:S(2)}) collective-permute-start(bf16[512,512]{1,0:T(8,128)(2,1)S(1)} %multiply_convert_fusion.own), channel_id=1, source_target_pairs={{0,2},{1,3},{2,0},{3,1},{4,6},{5,7},{6,4},{7,5},{8,10},{9,11},{10,... | collective-permute-start | bytes 1572872 | tf_op jit(solution)/shard_map/ppermute | solution.py:150
  63.0 2.6 %copy-start.5 = (bf16[512,512]{1,0:T(8,128)(2,1)}, bf16[512,512]{1,0:T(8,128)(2,1)S(1)}, u32[]{:S(2)}) copy-start(bf16[512,512]{1,0:T(8,128)(2,1)S(1)} %collective-permute-done.2.across) | copy-start | bytes 1572868
  63.0 2.6 %collective-permute-start.3 = (bf16[512,512]{1,0:T(8,128)(2,1)}, bf16[512,512]{1,0:T(8,128)(2,1)}, u32[]{:S(2)}, u32[]{:S(2)}) collective-permute-start(bf16[512,512]{1,0:T(8,128)(2,1)} %collective-permute-done.1.beside), channel_id=1, source_target_pairs={{0,1},{1,0},{2,3},{3,2},{4,5},{5,4},{6,7},{7,6},{8,9},{9,8},{10,11... | collective-permute-start | bytes 1572872 | tf_op jit(solution)/shard_map/ppermute | solution.py:158
  65.6 7.8 %copy-start.2 = (bf16[256,512]{1,0:T(8,128)(2,1)S(1)}, bf16[256,512]{1,0:T(8,128)(2,1)}, u32[]{:S(2)}) copy-start(bf16[256,512]{1,0:T(8,128)(2,1)} %mixer_gated.1.own) | copy-start | bytes 786436
  69.9 18.7 %all-to-all-start.3 = ((bf16[8,64,512]{2,1,0:T(8,128)(2,1)}), bf16[8,64,512]{2,1,0:T(8,128)(2,1)S(1)}, u32[]{:S(2)}, u32[]{:S(2)}) async-start(bf16[8,64,512]{2,1,0:T(8,128)(2,1)} %bitcast.29), calls=%async_computation.3 | async-start | bytes 1048576 | tf_op jit(solution)/shard_map/all_to_all | solution.py:327
  73.4 8.7 %collective-permute-start.4 = (bf16[256,512]{1,0:T(8,128)(2,1)S(1)}, bf16[256,512]{1,0:T(8,128)(2,1)S(1)}, u32[]{:S(2)}, u32[]{:S(2)}) collective-permute-start(bf16[256,512]{1,0:T(8,128)(2,1)S(1)} %copy-done.2), channel_id=1, source_target_pairs={{0,2},{1,3},{2,0},{3,1},{4,6},{5,7},{6,4},{7,5},{8,10},{9,11},{10,... | collective-permute-start | bytes 786440 | tf_op jit(solution)/shard_map/ppermute | solution.py:150
  74.4 7.6 %collective-permute-start.5 = (bf16[256,512]{1,0:T(8,128)(2,1)S(1)}, bf16[256,512]{1,0:T(8,128)(2,1)S(1)}, u32[]{:S(2)}, u32[]{:S(2)}) collective-permute-start(bf16[256,512]{1,0:T(8,128)(2,1)S(1)} %copy-done.2), channel_id=1, source_target_pairs={{0,1},{1,0},{2,3},{3,2},{4,5},{5,4},{6,7},{7,6},{8,9},{9,8},{10,11... | collective-permute-start | bytes 786440 | tf_op jit(solution)/shard_map/ppermute | solution.py:151
  82.0 1.7 %copy-start.6 = (bf16[256,512]{1,0:T(8,128)(2,1)}, bf16[256,512]{1,0:T(8,128)(2,1)S(1)}, u32[]{:S(2)}) copy-start(bf16[256,512]{1,0:T(8,128)(2,1)S(1)} %collective-permute-done.4.beside) | copy-start | bytes 786436
  82.0 1.7 %collective-permute-start.6 = (bf16[256,512]{1,0:T(8,128)(2,1)S(1)}, bf16[256,512]{1,0:T(8,128)(2,1)}, u32[]{:S(2)}, u32[]{:S(2)}) collective-permute-start(bf16[256,512]{1,0:T(8,128)(2,1)S(1)} %collective-permute-done.4.beside), channel_id=1, source_target_pairs={{0,1},{1,0},{2,3},{3,2},{4,5},{5,4},{6,7},{7,6},{8,9},{9,8},{10,11... | collective-permute-start | bytes 786440 | tf_op jit(solution)/shard_map/ppermute | solution.py:158
  82.0 1.7 %copy-start.7 = (bf16[256,512]{1,0:T(8,128)(2,1)}, bf16[256,512]{1,0:T(8,128)(2,1)S(1)}, u32[]{:S(2)}) copy-start(bf16[256,512]{1,0:T(8,128)(2,1)S(1)} %collective-permute-done.5.across) | copy-start | bytes 786436
  88.6 0.8 copy-start.1

commit v3 on v2

--- a/solution.py
+++ b/solution.py
@@ -11,6 +11,7 @@
 VDIM = 128
 GROUPS = 4
 TOPK = 2
+WAVES = 2
 
 norm_eps = 1e-06
 f32 = jnp.float32
@@ -194,22 +195,27 @@
     return named, jnp.where(member, counts.astype(jnp.int32), -1)
 
 
-def dispatch_kernel(place, tokens, gain, routes, out, *, capacity):
+def dispatch_kernel(place, tokens, gain, routes, *outs, slots):
     features = tokens[...].astype(f32)
     scale = lax.rsqrt(jnp.mean(features * features, axis=-1, keepdims=True) + norm_eps)
     normed = (features * scale * gain[...]).astype(bf16)
-    half = out.shape[1]
+    half = outs[0].shape[1]
     mine = jnp.where(place[0] == 0, normed[:, :half], normed[:, half:])
-    experts = out.shape[0] // capacity
+    experts = outs[0].shape[0] // slots
     _, ranks = slot_ranks(routes[...], experts)
-    slot = lax.broadcasted_iota(jnp.int32, (capacity, tokens.shape[0]), 0)
-    for e in range(experts):
-        pick = jnp.where(ranks[e : e + 1, :] == slot, 1.0, 0.0).astype(bf16)
-        out[e * capacity : (e + 1) * capacity, :] = dot(pick, mine, 1, 0).astype(bf16)
-
-
-def combine_kernel(routes, group_logits, choice_logits, values, out, *, capacity):
-    experts = values.shape[0] // capacity
+    slot = lax.broadcasted_iota(jnp.int32, (slots, tokens.shape[0]), 0)
+    for wave, out in enumerate(outs):
+        picks = [
+            jnp.where(ranks[e : e + 1, :] == slot + wave * slots, 1.0, 0.0)
+            for e in range(experts)
+        ]
+        pick = jnp.concatenate(picks, axis=0).astype(bf16)
+        out[...] = dot(pick, mine, 1, 0).astype(bf16)
+
+
+def combine_kernel(routes, group_logits, choice_logits, *refs, slots):
+    out = refs[-1]
+    experts = refs[0].shape[0] // slots
     tokens = routes.shape[1]
     chosen = routes[...]
     named, ranks = slot_ranks(chosen, experts)
@@ -228,35 +234,36 @@
             within += jnp.where(groups_of[i] == groups_of[j], choice_exp[i : i + 1, :], 0.0)
         weight = prob * choice_exp[j : j + 1, :] / within
         spread = jnp.where(named[j], weight, spread)
-    slot = lax.broadcasted_iota(jnp.int32, (capacity, tokens), 0)
-    mix = jnp.concatenate(
-        [
-            jnp.where(ranks[e : e + 1, :] == slot, spread[e : e + 1, :], 0.0)
+    slot = lax.broadcasted_iota(jnp.int32, (slots, tokens), 0)
+    total = jnp.zeros(out.shape, f32)
+    for wave, values in enumerate(refs[:-1]):
+        rows = [
+            jnp.where(ranks[e : e + 1, :] == slot + wave * slots, spread[e : e + 1, :], 0.0)
             for e in range(experts)
-        ],
-        axis=0,
-    )
-    high = mix.astype(bf16)
-    low = (mix - high.astype(f32)).astype(bf16)
-    out[...] = (dot(high, values[...], 0, 0) + dot(low, values[...], 0, 0)).astype(bf16)
+        ]
+        mix = jnp.concatenate(rows, axis=0)
+        high = mix.astype(bf16)
+        low = (mix - high.astype(f32)).astype(bf16)
+        total += dot(high, values[...], 0, 0) + dot(low, values[...], 0, 0)
+    out[...] = total.astype(bf16)
 
 
 def expert_dispatch(expert_tokens, expert_gain, routes):
     count, width = expert_tokens.shape
     experts = lax.axis_size("ep")
-    capacity = 2 * TOPK * count // experts
+    slots = 2 * TOPK * count // experts // WAVES
     half = width // 2
     core = (lax.axis_index("tp") % 2).astype(jnp.int32).reshape(1)
     vmem = pl.BlockSpec(memory_space=pltpu.VMEM)
     outgoing = pl.pallas_call(
-        functools.partial(dispatch_kernel, capacity=capacity),
+        functools.partial(dispatch_kernel, slots=slots),
         in_specs=[pl.BlockSpec(memory_space=pltpu.SMEM), vmem, vmem, vmem],
-        out_specs=vmem,
-        out_shape=jax.ShapeDtypeStruct((experts * capacity, half), bf16),
+        out_specs=[vmem] * WAVES,
+        out_shape=[jax.ShapeDtypeStruct((experts * slots, half), bf16)] * WAVES,
         cost_estimate=work(4),
         name="expert_dispatch",
     )(core, expert_tokens, expert_gain.reshape(1, width), routes.T)
-    return outgoing.reshape(experts, capacity, half)
+    return [wave.reshape(experts, slots, half) for wave in outgoing]
 
 
 def expert_hidden(arrived, w_gate, w_up):
@@ -274,14 +281,14 @@
 
 
 def expert_combine(came_back, routes, group_logits, choice_logits):
-    slots, width = came_back.shape
+    slots, width = came_back[0].shape
     count = routes.shape[0]
     return pl.pallas_call(
-        functools.partial(combine_kernel, capacity=slots // lax.axis_size("ep")),
+        functools.partial(combine_kernel, slots=slots // lax.axis_size("ep")),
         out_shape=jax.ShapeDtypeStruct((count, width), bf16),
         cost_estimate=work(3),
         name="expert_combine",
-    )(routes.T, group_logits.T, choice_logits.T, came_back)
+    )(routes.T, group_logits.T, choice_logits.T, *came_back)
 
 
 def per_device(
@@ -306,28 +313,35 @@
     heads = mixer_query.shape[1] // KEYDIM
     outgoing = expert_dispatch(expert_tokens, expert_gain, routes)
     outgoing, mixer_query = together((outgoing, mixer_query))
-    arrived = lax.all_to_all(outgoing, "ep", split_axis=0, concat_axis=0, tiled=True)
+    swap = lambda x: lax.all_to_all(x, "ep", split_axis=0, concat_axis=0, tiled=True)
+    arrived, arrived_last = swap(outgoing[0]), swap(outgoing[1])
     local, entry_query, packed = mixer_scan(
         mixer_query, mixer_forget, mixer_value, forget_floor, parts
     )
     arrived, packed = together((arrived, packed))
-    slices = lax.all_to_all(packed, "ep", split_axis=0, concat_axis=0, tiled=True)
     hidden = expert_hidden(arrived, w_gate[0], w_up[0])
-    hidden, slices = together((hidden, slices))
     pieces = spread_first(hidden)
-    prefixes = state_prefix(slices, heads)
-    entering = lax.all_to_all(prefixes, "ep", split_axis=0, concat_axis=0, tiled=True)
-    pieces, entering = together((pieces, entering))
-    pieces = spread_last(pieces)
+    packed, arrived_last, _ = together((packed, arrived_last, pieces))
+    slices = swap(packed)
+    hidden_last = expert_hidden(arrived_last, w_gate[0], w_up[0])
+    pieces_last = spread_first(hidden_last)
+    slices, pieces, _ = together((slices, pieces, hidden_last))
+    entering = swap(state_prefix(slices, heads))
+
+    def product(pieces):
+        return spread_dot(spread_last(pieces), w_down[0])
+
+    def send_back(values):
+        return swap(values.reshape(parts, -1, values.shape[1])).reshape(values.shape)
+
+    values, entering = together((product(pieces), entering))
+    came_back = send_back(values)
     mixed = mixer_gated(local, entry_query, entering, mixer_gate, head_gain)
-    pieces, mixed = together((pieces, mixed))
-    mixed_pieces = spread_first(mixed)
-    values = spread_dot(pieces, w_down[0])
-    shaped = values.reshape(arrived.shape[0], arrived.shape[1], values.shape[1])
-    came_back = lax.all_to_all(shaped, "ep", split_axis=0, concat_axis=0, tiled=True)
-    mixer_out = spread_dot(spread_last(mixed_pieces), mixer_proj)
-    came_back, mixer_out = together((came_back, mixer_out))
-    came_back = came_back.reshape(values.shape)
+    pieces_last, mixed = together((pieces_last, mixed))
+    came_last = send_back(product(pieces_last))
+    mixer_out = spread_dot(spread_last(spread_first(mixed)), mixer_proj)
+    came_back, came_last, mixer_out = together((came_back, came_last, mixer_out))
+    came_back = (came_back, came_last)
     expert_out = expert_combine(came_back, routes, group_logits, choice_logits)
     return (mixer_out, expert_out)
 

time: 92.3 us -> 100 us (1.083)
  starting transfers between devices: 17.3 us -> 31.5 us
  blocking collectives: 11.6 us -> 0 us
  local copies, waits for them, and re-layouts: 1.17 us -> 5.55 us
  Pallas kernels: 20.5 us -> 22.5 us
  waiting for transfers between devices: 36.3 us -> 34.7 us
    all_to_all x1 -> x0, blocking collectives: 11.6 us -> none  [per_device(): lax.all_to_all(prefixes, 'ep', split_axis=0, concat_axis=0, tiled=True)]
    all_to_all x3 -> x6, starting transfers between devices: 14.4 us -> 25.7 us  [per_device(): lax.all_to_all(x, 'ep', split_axis=0, concat_axis=0, tiled=True)]
    ppermute x2 -> x3, waiting for transfers between devices: 7.37 us -> 0.01 us  [spread_first(): beside = lax.ppermute(part, 'tp', [(i, i ^ 2) for i in range(4)])]
    all_to_all x3 -> x6, waiting for transfers between devices: 27.3 us -> 33 us  [per_device(): lax.all_to_all(x, 'ep', split_axis=0, concat_axis=0, tiled=True)]
    unnamed x18 -> x32, local copies, waits for them, and re-layouts: 1.17 us -> 5.55 us
    pallas_call x2 -> x3, Pallas kernels: 7.49 us -> 9.74 us  [spread_dot(): pl.pallas_call(four_parts_kernel, grid_spec=pltpu.PrefetchScalarGridSpec(...]
    ppermute x2 -> x3, starting transfers between devices: 2.58 us -> 4.68 us  [spread_first(): beside = lax.ppermute(part, 'tp', [(i, i ^ 2) for i in range(4)])]
    ppermute x2 -> x3, waiting for transfers between devices: 0.01 us -> 1.03 us  [spread_first(): across = lax.ppermute(part, 'tp', [(i, i ^ 1) for i in range(4)])]
  transfers between devices with their start and end apart: 10 -> 17, of which waited for: 5 -> 9; matrix products, arithmetic and copies ran while one was open for 4% -> 4% of each run, Pallas kernels for 12% -> 18%
where the time goes in v3:
time: 100 us; the launch traced here: 99.3 us
  waiting for transfers between devices  34.7 us (35%)
  starting transfers between devices  31.5 us (32%)
  Pallas kernels  22.5 us (22%)
  local copies, waits for them, and re-layouts  5.55 us (6%)
  matrix products  2.9 us (3%)
  other arithmetic  1.22 us (1%)
    all_to_all x6, waiting for transfers between devices, per_device(): lax.all_to_all(x, 'ep', split_axis=0, concat_axis=0, tiled=True)  33 us
    all_to_all x6, starting transfers between devices, per_device(): lax.all_to_all(x, 'ep', split_axis=0, concat_axis=0, tiled=True)  25.7 us
    pallas_call x3, Pallas kernels, spread_dot(): pl.pallas_call(four_parts_kernel, grid_spec=pltpu.PrefetchScalarGridSpec(...  9.74 us
    unnamed x32, local copies, waits for them, and re-layouts  5.55 us
    ppermute x3, starting transfers between devices, spread_first(): beside = lax.ppermute(part, 'tp', [(i, i ^ 2) for i in range(4)])  4.68 us
    pallas_call x1, Pallas kernels, mixer_scan(): pl.pallas_call(functools.partial(mixer_scan_kernel, rows=rows, base=base)...  3.87 us
    pallas_call x1, Pallas kernels, expert_dispatch(): pl.pallas_call(functools.partial(dispatch_kernel, slots=slots), in_specs=...  2.7 us
    pallas_call x1, Pallas kernels, mixer_gated(): pl.pallas_call(mixer_gate_kernel, out_shape=jax.ShapeDtypeStruct((length,...  2.39 us
  transfers between devices with their start and end apart: 17, of which 9 were waited for; matrix products, arithmetic and copies ran while one was open for 4% of the time, Pallas kernels for 18%

profile of v3, /device:TPU:0, one launch (start us, length us, event | category | flops | bytes accessed | tf_op | source)
XLA Modules:
  0.0 99.3 jit_solution(3227599507968390354)
XLA Ops:
  0.7 2.7 %expert_dispatch.1 = (bf16[256,1024]{1,0:T(8,128)(2,1)}, bf16[256,1024]{1,0:T(8,128)(2,1)}) custom-call(s32[1]{0:T(128)} %bitcast.1.place, bf16[128,2048]{1,0:T(8,128)(2,1)} %tokens.1, f32[1,2048]{1,0:T(1,128)} %bitcast.56, s32[2,128]{1,0:T(2,128)} %bitcast.52), custom_call_target="tpu_custom_call" | custom-call | flops 200000000 | tf_op jit(solution)/shard_map/expert_dispatch/pallas_call | solution.py:258
  3.4 7.3 %all-to-all-start = ((bf16[8,32,1024]{2,1,0:T(8,128)(2,1)}), bf16[8,32,1024]{2,1,0:T(8,128)(2,1)S(1)}, u32[]{:S(2)}, u32[]{:S(2)}) async-start(bf16[8,32,1024]{2,1,0:T(8,128)(2,1)} %bitcast.50), calls=%async_computation | async-start | bytes 1048576 | tf_op jit(solution)/shard_map/all_to_all | solution.py:316
  10.6 3.9 %mixer_scan.1 = (f32[256,512]{1,0:T(8,128)}, bf16[256,512]{1,0:T(8,128)(2,1)}, bf16[8,80,128]{2,1,0:T(8,128)(2,1)}) custom-call(bf16[256,512]{1,0:T(8,128)(2,1)} %query, bf16[256,512]{1,0:T(8,128)(2,1)} %forget.1, bf16[256,512]{1,0:T(8,128)(2,1)} %value.1, f32[1,512]{1,0:T(1,128)} %bitcast.57), custom_call_target="tpu_custom_call" | custom-call | flops 400000000 | tf_op jit(solution)/shard_map/mixer_scan/pallas_call | solution.py:76
  14.5 10.6 %all-to-all-done = bf16[8,32,1024]{2,1,0:T(8,128)(2,1)S(1)} async-done(((bf16[8,32,1024]{2,1,0:T(8,128)(2,1)}), bf16[8,32,1024]{2,1,0:T(8,128)(2,1)S(1)}, u32[]{:S(2)}, u32[]{:S(2)}) %all-to-all-start) | async-done | bytes 524320 | tf_op jit(solution)/shard_map/all_to_all | solution.py:316
  25.1 3.6 %all-to-all-start.1 = ((bf16[8,32,1024]{2,1,0:T(8,128)(2,1)}), bf16[8,32,1024]{2,1,0:T(8,128)(2,1)S(1)}, u32[]{:S(2)}, u32[]{:S(2)}) async-start(bf16[8,32,1024]{2,1,0:T(8,128)(2,1)} %bitcast.49), calls=%async_computation.1 | async-start | bytes 1048576 | tf_op jit(solution)/shard_map/all_to_all | solution.py:316
  28.8 1.1 %broadcast_select_fusion.3 = (bf16[256,1024]{1,0:T(8,128)(2,1)S(1)}, bf16[256,1024]{1,0:T(8,128)(2,1)S(1)}) fusion(bf16[256,1024]{1,0:T(8,128)(2,1)} %collective-permute-done, pred[]{:T(512)S(6)} %eq.8, bf16[8,32,1024]{2,1,0:T(8,128)(2,1)S(1)} %all-to-all-done), kind=kLoop, calls=%fused_computation.15 | loop fusion | flops 524288 | bytes 2097153 | tf_op jit(solution)/shard_map/jit(_where)/select_n | solution.py:276
  32.7 1.5 %collective-permute-start.1 = (bf16[256,512]{1,0:T(8,128)(2,1)S(1)}, bf16[256,512]{1,0:T(8,128)(2,1)S(1)}, u32[]{:S(2)}, u32[]{:S(2)}) collective-permute-start(bf16[256,512]{1,0:T(8,128)(2,1)S(1)} %multiply_convert_fusion.1.own), channel_id=1, source_target_pairs={{0,2},{1,3},{2,0},{3,1},{4,6},{5,7},{6,4},{7,5},{8,10},{9,11},{10,... | collective-permute-start | bytes 786440 | tf_op jit(solution)/shard_map/ppermute | solution.py:151
  34.2 9.8 %all-to-all-done.1 = bf16[8,32,1024]{2,1,0:T(8,128)(2,1)S(1)} async-done(((bf16[8,32,1024]{2,1,0:T(8,128)(2,1)}), bf16[8,32,1024]{2,1,0:T(8,128)(2,1)S(1)}, u32[]{:S(2)}, u32[]{:S(2)}) %all-to-all-start.1) | async-done | bytes 524320 | tf_op jit(solution)/shard_map/all_to_all | solution.py:316
  45.4 3.7 %all-to-all-start.2 = ((bf16[8,80,128]{2,1,0:T(8,128)(2,1)}), bf16[8,80,128]{2,1,0:T(8,128)(2,1)S(1)}, u32[]{:S(2)}, u32[]{:S(2)}) async-start(bf16[8,80,128]{2,1,0:T(8,128)(2,1)} %get-tuple-element.35), calls=%async_computation.2 | async-start | bytes 327680 | tf_op jit(solution)/shard_map/all_to_all | solution.py:316
  51.5 5.6 %all-to-all-done.2.packed = bf16[8,80,128]{2,1,0:T(8,128)(2,1)S(1)} async-done(((bf16[8,80,128]{2,1,0:T(8,128)(2,1)}), bf16[8,80,128]{2,1,0:T(8,128)(2,1)S(1)}, u32[]{:S(2)}, u32[]{:S(2)}) %all-to-all-start.2) | async-done | bytes 163872 | tf_op jit(solution)/shard_map/all_to_all | solution.py:316
  57.8 1.6 %state_prefix.1 = bf16[8,64,128]{2,1,0:T(8,128)(2,1)} custom-call(bf16[8,80,128]{2,1,0:T(8,128)(2,1)} %copy-done.4), custom_call_target="tpu_custom_call" | custom-call | flops 50000000 | tf_op jit(solution)/shard_map/state_prefix/pallas_call | solution.py:106
  59.4 3.4 %all-to-all-start.3 = ((bf16[8,64,128]{2,1,0:T(8,128)(2,1)}), bf16[8,64,128]{2,1,0:T(8,128)(2,1)S(1)}, u32[]{:S(2)}, u32[]{:S(2)}) async-start(bf16[8,64,128]{2,1,0:T(8,128)(2,1)} %state_prefix.1), calls=%async_computation.3 | async-start | bytes 262144 | tf_op jit(solution)/shard_map/all_to_all | solution.py:316
  62.9 1.6 %collective-permute-start.5 = (bf16[256,512]{1,0:T(8,128)(2,1)S(1)}, bf16[256,512]{1,0:T(8,128)(2,1)}, u32[]{:S(2)}, u32[]{:S(2)}) collective-permute-start(bf16[256,512]{1,0:T(8,128)(2,1)S(1)} %multiply_convert_fusion.own), channel_id=1, source_target_pairs={{0,2},{1,3},{2,0},{3,1},{4,6},{5,7},{6,4},{7,5},{8,10},{9,11},{10,... | collective-permute-start | bytes 786440 | tf_op jit(solution)/shard_map/ppermute | solution.py:151
  64.5 3.2 %spread_dot.3 = bf16[256,512]{1,0:T(8,128)(2,1)} custom-call(s32[1]{0:T(128)} %bitcast.place, bf16[256,512]{1,0:T(8,128)(2,1)} %copy-done.6, bf16[256,512]{1,0:T(8,128)(2,1)} %copy-done.9, bf16[256,512]{1,0:T(8,128)(2,1)} %copy-done.7, bf16[256,512]{1,0:T(8,128)(2,1)} %collective-permute-done.4.last, bf16[2048,512]{1,0:T(8,128)(2,1)} %bitcast.35, ...), custom_call_target="tpu_custom_call" | custom-call | flops 200000000 | tf_op jit(solution)/shard_map/spread_dot/pallas_call | solution.py:171
  67.7 2.4 %all-to-all-done.3.entering = bf16[8,64,128]{2,1,0:T(8,128)(2,1)S(1)} async-done(((bf16[8,64,128]{2,1,0:T(8,128)(2,1)}), bf16[8,64,128]{2,1,0:T(8,128)(2,1)S(1)}, u32[]{:S(2)}, u32[]{:S(2)}) %all-to-all-start.3) | async-done | bytes 131104 | tf_op jit(solution)/shard_map/all_to_all | solution.py:316
  70.1 3.4 %all-to-all-start.4 = ((bf16[8,32,512]{2,1,0:T(8,128)(2,1)}), bf16[8,32,512]{2,1,0:T(8,128)(2,1)S(1)}, u32[]{:S(2)}, u32[]{:S(2)}) async-start(bf16[8,32,512]{2,1,0:T(8,128)(2,1)} %bitcast.45), calls=%async_computation.4 | async-start | bytes 524288 | tf_op jit(solution)/shard_map/all_to_all | solution.py:316
  73.5 2.4 %mixer_gated.1.own = bf16[256,512]{1,0:T(8,128)(2,1)} custom-call(f32[256,512]{1,0:T(8,128)} %get-tuple-element.42.local, bf16[256,512]{1,0:T(8,128)(2,1)} %get-tuple-element.43.entry_query, bf16[8,64,128]{2,1,0:T(8,128)(2,1)} %copy-done.5, bf16[256,512]{1,0:T(8,128)(2,1)} %gate.1, f32[1,128]{1,0:T(1,128)} %bitcast.55), custom_call_target="tpu_custom_call" | custom-call | flops 150000000 | tf_op jit(solution)/shard_map/mixer_gated/pallas_call | solution.py:132
  76.0 1.6 %collective-permute-start.8 = (bf16[256,512]{1,0:T(8,128)(2,1)}, bf16[256,512]{1,0:T(8,128)(2,1)}, u32[]{:S(2)}, u32[]{:S(2)}) collective-permute-start(bf16[256,512]{1,0:T(8,128)(2,1)} %mixer_gated.1.own), channel_id=1, source_target_pairs={{0,2},{1,3},{2,0},{3,1},{4,6},{5,7},{6,4},{7,5},{8,10},{9,11},{10,... | collective-permute-start | bytes 786440 | tf_op jit(solution)/shard_map/ppermute | solution.py:151
  77.9 3.2 %spread_dot.4 = bf16[256,512]{1,0:T(8,128)(2,1)} custom-call(s32[1]{0:T(128)} %bitcast.place, bf16[256,512]{1,0:T(8,128)(2,1)} %copy-done.8, bf16[256,512]{1,0:T(8,128)(2,1)} %collective-permute-done.5.beside, bf16[256,512]{1,0:T(8,128)(2,1)} %copy-done.11, bf16[256,512]{1,0:T(8,128)(2,1)} %collective-permute-done.7.last, bf16[2048,512]{1,0:T(8,128)(2,1)} %bitcast.39, ...), custom_call_target="tpu_custom_call" | custom-call | flops 200000000 | tf_op jit(solution)/shard_map/spread_dot/pallas_call | solution.py:171
  81.1 1.7 %all-to-all-done.4 = bf16[8,32,512]{2,1,0:T(8,128)(2,1)S(1)} async-done(((bf16[8,32,512]{2,1,0:T(8,128)(2,1)}), bf16[8,32,512]{2,1,0:T(8,128)(2,1)S(1)}, u32[]{:S(2)}, u32[]{:S(2)}) %all-to-all-start.4) | async-done | bytes 262176 | tf_op jit(solution)/shard_map/all_to_all | solution.py:316
  82.9 4.3 %all-to-all-start.5 = ((bf16[8,32,512]{2,1,0:T(8,128)(2,1)}), bf16[8,32,512]{2,1,0:T(8,128)(2,1)S(1)}, u32[]{:S(2)}, u32[]{:S(2)}) async-start(bf16[8,32,512]{2,1,0:T(8,128)(2,1)} %bitcast.46), calls=%async_computation.5 | async-start | bytes 524288 | tf_op jit(solution)/shard_map/all_to_all | solution.py:316
  90.2 3.2 %spread_dot.5 = bf16[256,512]{1,0:T(8,128)(2,1)} custom-call(s32[1]{0:T(128)} %bitcast.place, bf16[256,512]{1,0:T(8,128)(2,1)} %mixer_gated.1.own, bf16[256,512]{1,0:T(8,128)(2,1)} %collective-permute-done.8.beside, bf16[256,512]{1,0:T(8,128)(2,1)} %copy-done.12, bf16[256,512]{1,0:T(8,128)(2,1)} %copy-done.13, bf16[2048,512]{1,0:T(8,128)(2,1)} %w3.1, ...), custom_call_target="tpu_custom_call" | custom-call | flops 200000000 | tf_op jit(solution)/shard_map/spread_dot/pallas_call | solution.py:171
  93.4 2.9 %all-to-all-done.5 = bf16[8,32,512]{2,1,0:T(8,128)(2,1)S(1)} async-done(((bf16[8,32,512]{2,1,0:T(8,128)(2,1)}), bf16[8,32,512]{2,1,0:T(8,128)(2,1)S(1)}, u32[]{:S(2)}, u32[]{:S(2)}) %all-to-all-start.5) | async-done | bytes 262176 | tf_op jit(solution)/shard_map/all_to_all | solution.py:316
  97.1 2.2 %expert_combine.1 = bf16[128,512]{1,0:T(8,128)(2,1)} custom-call(s32[2,128]{1,0:T(2,128)} %bitcast.53, f32[4,128]{1,0:T(4,128)} %bitcast.51, f32[2,128]{1,0:T(2,128)} %bitcast.54, bf16[256,512]{1,0:T(8,128)(2,1)} %bitcast.47, bf16[256,512]{1,0:T(8,128)(2,1)} %bitcast.48), custom_call_target="tpu_custom_call" | custom-call | flops 150000000 | tf_op jit(solution)/shard_map/expert_combine/pallas_call | solution.py:286
  (56 shorter events, 11.4 us)
Async XLA Ops:
  0.6 29.3 %copy-start = (bf16[1,2048,512]{2,1,0:T(8,128)(2,1)S(1)}, bf16[1,2048,512]{2,1,0:T(8,128)(2,1)}, u32[]{:S(2)}) copy-start(bf16[1,2048,512]{2,1,0:T(8,128)(2,1)} %param.27) | copy-start | bytes 6291460
  3.4 21.8 %all-to-all-start = ((bf16[8,32,1024]{2,1,0:T(8,128)(2,1)}), bf16[8,32,1024]{2,1,0:T(8,128)(2,1)S(1)}, u32[]{:S(2)}, u32[]{:S(2)}) async-start(bf16[8,32,1024]{2,1,0:T(8,128)(2,1)} %bitcast.50), calls=%async_computation | async-start | bytes 1048576 | tf_op jit(solution)/shard_map/all_to_all | solution.py:316
  25.1 3.7 %collective-permute-start = (bf16[256,1024]{1,0:T(8,128)(2,1)S(1)}, bf16[256,1024]{1,0:T(8,128)(2,1)}, u32[]{:S(2)}, u32[]{:S(2)}) collective-permute-start(bf16[256,1024]{1,0:T(8,128)(2,1)S(1)} %bitcast.44), channel_id=1, source_target_pairs={{0,1},{1,0},{2,3},{3,2},{4,5},{5,4},{6,7},{7,6},{8,9},{9,8},{10,11... | collective-permute-start | bytes 1572872 | tf_op jit(solution)/shard_map/ppermute | solution.py:273
  25.1 18.9 %all-to-all-start.1 = ((bf16[8,32,1024]{2,1,0:T(8,128)(2,1)}), bf16[8,32,1024]{2,1,0:T(8,128)(2,1)S(1)}, u32[]{:S(2)}, u32[]{:S(2)}) async-start(bf16[8,32,1024]{2,1,0:T(8,128)(2,1)} %bitcast.49), calls=%async_computation.1 | async-start | bytes 1048576 | tf_op jit(solution)/shard_map/all_to_all | solution.py:316
  32.2 11.8 %copy-start.6 = (bf16[256,512]{1,0:T(8,128)(2,1)}, bf16[256,512]{1,0:T(8,128)(2,1)S(1)}, u32[]{:S(2)}) copy-start(bf16[256,512]{1,0:T(8,128)(2,1)S(1)} %multiply_convert_fusion.1.own) | copy-start | bytes 786436
  32.2 11.7 %collective-permute-start.2 = (bf16[256,512]{1,0:T(8,128)(2,1)S(1)}, bf16[256,512]{1,0:T(8,128)(2,1)S(1)}, u32[]{:S(2)}, u32[]{:S(2)}) collective-permute-start(bf16[256,512]{1,0:T(8,128)(2,1)S(1)} %multiply_convert_fusion.1.own), channel_id=1, source_target_pairs={{0,1},{1,0},{2,3},{3,2},{4,5},{5,4},{6,7},{7,6},{8,9},{9,8},{10,11... | collective-permute-start | bytes 786440 | tf_op jit(solution)/shard_map/ppermute | solution.py:152
  32.7 11.3 %collective-permute-start.1 = (bf16[256,512]{1,0:T(8,128)(2,1)S(1)}, bf16[256,512]{1,0:T(8,128)(2,1)S(1)}, u32[]{:S(2)}, u32[]{:S(2)}) collective-permute-start(bf16[256,512]{1,0:T(8,128)(2,1)S(1)} %multiply_convert_fusion.1.own), channel_id=1, source_target_pairs={{0,2},{1,3},{2,0},{3,1},{4,6},{5,7},{6,4},{7,5},{8,10},{9,11},{10,... | collective-permute-start | bytes 786440 | tf_op jit(solution)/shard_map/ppermute | solution.py:151
  45.4 3.7 %collective-permute-start.3 = (bf16[256,1024]{1,0:T(8,128)(2,1)S(1)}, bf16[256,1024]{1,0:T(8,128)(2,1)S(1)}, u32[]{:S(2)}, u32[]{:S(2)}) collective-permute-start(bf16[256,1024]{1,0:T(8,128)(2,1)S(1)} %bitcast.43), channel_id=1, source_target_pairs={{0,1},{1,0},{2,3},{3,2},{4,5},{5,4},{6,7},{7,6},{8,9},{9,8},{10,11... | collective-permute-start | bytes 1572872 | tf_op jit(solution)/shard_map/ppermute | solution.py:273
  45.4 11.8 %all-to-all-start.2 = ((bf16[8,80,128]{2,1,0:T(8,128)(2,1)}), bf16[8,80,128]{2,1,0:T(8,128)(2,1)S(1)}, u32[]{:S(2)}, u32[]{:S(2)}) async-start(bf16[8,80,128]{2,1,0:T(8,128)(2,1)} %get-tuple-element.35), calls=%async_computation.2 | async-start | bytes 327680 | tf_op jit(solution)/shard_map/all_to_all | solution.py:316
  50.8 6.4 %copy-start.10 = (bf16[256,512]{1,0:T(8,128)(2,1)S(1)}, bf16[256,512]{1,0:T(8,128)(2,1)}, u32[]{:S(2)}) copy-start(bf16[256,512]{1,0:T(8,128)(2,1)} %copy-done.9) | copy-start | bytes 786436
  51.5 26.4 %copy-start.8 = (bf16[256,512]{1,0:T(8,128)(2,1)}, bf16[256,512]{1,0:T(8,128)(2,1)S(1)}, u32[]{:S(2)}) copy-start(bf16[256,512]{1,0:T(8,128)(2,1)S(1)} %multiply_convert_fusion.own) | copy-start | bytes 786436
  57.2 7.3 %collective-permute-start.4 = (bf16[256,512]{1,0:T(8,128)(2,1)S(1)}, bf16[256,512]{1,0:T(8,128)(2,1)}, u32[]{:S(2)}, u32[]{:S(2)}) collective-permute-start(bf16[256,512]{1,0:T(8,128)(2,1)S(1)} %copy-done.10), channel_id=1, source_target_pairs={{0,1},{1,0},{2,3},{3,2},{4,5},{5,4},{6,7},{7,6},{8,9},{9,8},{10,11... | collective-permute-start | bytes 786440 | tf_op jit(solution)/shard_map/ppermute | solution.py:159
  59.4 10.7 %all-to-all-start.3 = ((bf16[8,64,128]{2,1,0:T(8,128)(2,1)}), bf16[8,64,128]{2,1,0:T(8,128)(2,1)S(1)}, u32[]{:S(2)}, u32[]{:S(2)}) async-start(bf16[8,64,128]{2,1,0:T(8,128)(2,1)} %state_prefix.1), calls=%async_computation.3 | async-start | bytes 262144 | tf_op jit(solution)/shard_map/all_to_all | solution.py:316
  62.8 13.1 %collective-permute-start.6 = (bf16[256,512]{1,0:T(8,128)(2,1)S(1)}, bf16[256,512]{1,0:T(8,128)(2,1)S(1)}, u32[]{:S(2)}, u32[]{:S(2)}) collective-permute-start(bf16[256,512]{1,0:T(8,128)(2,1)S(1)} %multiply_convert_fusion.own), channel_id=1, source_target_pairs={{0,1},{1,0},{2,3},{3,2},{4,5},{5,4},{6,7},{7,6},{8,9},{9,8},{10,11... | collective-permute-start | bytes 786440 | tf_op jit(solution)/shard_map/ppermute | solution.py:152
  62.9 13.0 %collective-permute-start.5 = (bf16[256,512]{1,0:T(8,128)(2,1)S(1)}, bf16[256,512]{1,0:T(8,128)(2,1)}, u32[]{:S(2)}, u32[]{:S(2)}) collective-permute-start(bf16[256,512]{1,0:T(8,128)(2,1)S(1)} %multiply_convert_fusion.own), channel_id=1, source_target_pairs={{0,2},{1,3},{2,0},{3,1},{4,6},{5,7},{6,4},{7,5},{8,10},{9,11},{10,... | collective-permute-start | bytes 786440 | tf_op jit(solution)/shard_map/ppermute | solution.py:151
  70.1 3.4 %copy-start.5 = (bf16[8,64,128]{2,1,0:T(8,128)(2,1)}, bf16[8,64,128]{2,1,0:T(8,128)(2,1)S(1)}, u32[]{:S(2)}) copy-start(bf16[8,64,128]{2,1,0:T(8,128)(2,1)S(1)} %all-to-all-done.3.entering) | copy-start | bytes 393220
  70.1 12.7 %all-to-all-start.4 = ((bf16[8,32,512]{2,1,0:T(8,128)(2,1)}), bf16[8,32,512]{2,1,0:T(8,128)(2,1)S(1)}, u32[]{:S(2)}, u32[]{:S(2)}) async-start(bf16[8,32,512]{2,1,0:T(8,128)(2,1)} %bitcast.45), calls=%async_computation.4 | async-start | bytes 524288 | tf_op jit(solution)/shard_map/all_to_all | solution.py:316
  75.9 11.2 %copy-start.2 = (bf16[256,512]{1,0:T(8,128)(2,1)S(1)}, bf16[256,512]{1,0:T(8,128)(2,1)}, u32[]{:S(2)}) copy-start(bf16[256,512]{1,0:T(8,128)(2,1)} %mixer_gated.1.own) | copy-start | bytes 786436
  76.0 1.9 %collective-permute-start.7 = (bf16[256,512]{1,0:T(8,128)(2,1)}, bf16[256,512]{1,0:T(8,128)(2,1)}, u32[]{:S(2)}, u32[]{:S(2)}) collective-permute-start(bf16[256,512]{1,0:T(8,128)(2,1)} %collective-permute-done.5.beside), channel_id=1, source_target_pairs={{0,1},{1,0},{2,3},{3,2},{4,5},{5,4},{6,7},{7,6},{8,9},{9,8},{10,11... | collective-permute-start | bytes 786440 | tf_op jit(solution)/shard_map/ppermute | solution.py:159
  76.0 11.2 %collective-permute-start.8 = (bf16[256,512]{1,0:T(8,128)(2,1)}, bf16[256,512]{1,0:T(8,128)(2,1)}, u32[]{:S(2)}, u32[]{:S(2)}) collective-permute-start(bf16[256,512]{1,0:T(8,128)(2,1)} %mixer_gated.1.own), channel_id=1, source_target_pairs={{0,2},{1,3},{2,0},{3,1},{4,6},{5,7},{6,4},{7,5},{8,10},{9,11},{10,... | collective-permute-start | bytes 786440 | tf_op jit(solution)/shard_map/ppermute | solution.py:151
  82.9 10.6 %copy-start.1 = (bf16[8,32,512]{2,1,0:T(8,128)(2,1)}, bf16[8,32,512]{2,1,0:T(8,128)(2,1)S(1)}, u32[]{:S(2)}) copy-start(bf16[8,32,512]{2,1,0:T(8,128)(2,1)S(1)} %all-to-all-done.4) | copy-start | bytes 786436
  82.9 13.5 %all-to-all-start.5 = ((bf16[8,32,512]{2,1,0:T(8,128)(2,1)}), bf16[8,32,512]{2,1,0:T(8,128)(2,1)S(1)}, u32[]{:S(2)}, u32[]{:S(2)}) async-start(bf16[8,32,512]{2,1,0:T(8,128)(2,1)} %bitcast.46), calls=%async_computation.5 | async-start | bytes 524288 | tf_op jit(solution)/shard_map/all_to_all | solution.py:316
  87.2 1.6 %collective-permute-start.9 = (bf16[256,512]{1,0:T(8,128)(2,1)S(1)}, bf16[256,512]{1,0:T(8,128)(2,1)S(1)}, u32[]{:S(2)}, u32[]{:S(2)}) collective-permute-start(bf16[256,512]{1,0:T(8,128)(2,1)S(1)} %copy-done.2), channel_id=1, source_target_pairs={{0,1},{1,0},{2,3},{3,2},{4,5},{5,4},{6,7},{7,6},{8,9},{9,8},{10,11... | collective-permute-start | bytes 786440 | tf_op jit(solution)/shard_map/ppermute | solution.py:152
  87.3 1.9 %collective-permute-start.10 = (bf16[256,512]{1,0:T(8,128)(2,1)}, bf16[256,512]{1,0:T(8,128)(2,1)S(1)}, u32[]{:S(2)}, u32[]{:S(2)}) collective-permute-start(bf16[256,512]{1,0:T(8,128)(2,1)} %collective-permute-done.8.beside), channel_id=1, source_target_pairs={{0,1},{1,0},{2,3},{3,2},{4,5},{5,4},{6,7},{7,6},{8,9},{9,8},{10,11... | collective-permute-start | bytes 786440 | tf_op jit(solution)/shard_map/ppermute | solution.py:159
  (9 other events, 9.4 us)
